TPU v7x, 512 devices: a 4x2x32 block of a 4x8x32 slice. The times are simulated.
512 devices in a mesh: grp: 2 (over y), fs: 32 (over z), tp: 8 (over x, core).
Axes of the slice: x: 4, y: 2, z: 32, core: 2. Of those that a mesh axis runs over, the one named last changes fastest.
The devices are a block of a 4x8x32 slice.
Arguments:
- tokens: bfloat16 [24576, 2048], P(('grp', 'fs'), 'tp'), parts along dimension 0, may hold values from -6 to 6
- mix_gain: float32 [2048], replicated, may hold values from 0.1 to 1.9
- w_signal: bfloat16 [2048, 1024], P('fs', 'tp'), may hold values from -0.125 to 0.125
- w_outer_gate: bfloat16 [2048, 1024], P('fs', 'tp'), may hold values from -0.125 to 0.125
- w_inner_gate: bfloat16 [2048, 1024], P('fs', 'tp'), may hold values from -0.125 to 0.125
- mix_taps: float32 [3, 1024], P(None, 'tp'), may hold values from -3 to 3
- w_mix_out: bfloat16 [1024, 2048], P('tp', 'fs'), may hold values from -0.1875 to 0.1875
- ffn_gain: float32 [2048], replicated, may hold values from 0.1 to 1.9
- w_gate: bfloat16 [2048, 5120], P('fs', 'tp'), may hold values from -0.125 to 0.125
- w_value: bfloat16 [2048, 5120], P('fs', 'tp'), may hold values from -0.125 to 0.125
- up_taps: float32 [2, 3, 5120], P(None, None, 'tp'), may hold values from -3 to 3
- up_bias: float32 [2, 5120], P(None, 'tp'), may hold values from -3 to 3
- w_down: bfloat16 [5120, 2048], P('tp', 'fs'), may hold values from -0.078125 to 0.078125
Outputs:
- layer_out: bfloat16 [24576, 2048], P(('grp', 'fs'), 'tp'), parts along dimension 0
There are 2 independent parts, one for each index of `grp`. A program takes and returns all parts, laid end to end along the dimension named above; an argument that names none is the same for every part. Nothing has to cross between parts.
All inputs are finite; a program needn't handle non-finite values.
Results may differ from a plain program's by a relative error of at most 0.022.
Values may be sent and summed in bfloat16 or wider, within the bound.
No kernel may reach another device: no remote copies, remote signals or barrier semaphores. Data moves between devices by JAX's collectives and lax.ppermute only.
A program may use at most 64 MiB of HBM per device.

v0:
```python
import jax
import jax.numpy as jnp
from jax import lax
from jax.sharding import PartitionSpec as P

SEQS_DEV = 2


def in_one_piece(arrays, axis, dim, along):
    widths = [a.shape[along] for a in arrays]
    both = jnp.concatenate(arrays, axis=along)
    filled = lax.all_gather(both, axis, axis=dim, tiled=True)
    return tuple(jnp.split(filled, [sum(widths[:k]) for k in range(1, len(widths))], axis=along))


def copy_for_each(value, axis):
    copies = jnp.broadcast_to(value, (lax.axis_size(axis), *value.shape))
    return lax.all_to_all(copies, axis, split_axis=0, concat_axis=0, tiled=True)


def in_order(pieces, dim):
    shape = list(pieces.shape[1:])
    shape[dim] *= pieces.shape[0]
    return jnp.moveaxis(pieces, 0, dim).reshape(shape)


def gathered_copies(value, axis, dim):
    pieces = copy_for_each(value, axis)
    return in_order(pieces, dim)


def split_up(value, dim, devices):
    shape = value.shape
    pieces = value.reshape(*shape[:dim], devices, shape[dim] // devices, *shape[dim + 1 :])
    return jnp.moveaxis(pieces, dim, 0)


def sent_and_summed(value, axis, dim):
    devices = lax.axis_size(axis)
    pieces = lax.all_to_all(split_up(value, dim, devices), axis, 0, 0, tiled=True)
    return jnp.sum(pieces.astype(jnp.float32), axis=0)


def conv_positions(values, taps):
    width = values.shape[1]
    blocks = values.reshape(SEQS_DEV, -1, width)
    length = blocks.shape[1]
    padded = jnp.pad(blocks, ((0, 0), (2, 0), (0, 0)))
    result = (
        padded[:, 0:length] * taps[0]
        + padded[:, 1 : length + 1] * taps[1]
        + padded[:, 2 : length + 2] * taps[2]
    )
    return result.reshape(-1, width)


def rms_norm(stream, gain):
    values = stream.astype(jnp.float32)
    scale = lax.rsqrt(jnp.mean(values * values, axis=-1, keepdims=True) + 1e-06)
    return (values * scale * gain).astype(jnp.bfloat16)


def on_device(
    tokens,
    mix_gain,
    w_signal,
    w_outer_gate,
    w_inner_gate,
    mix_taps,
    w_mix_out,
    ffn_gain,
    w_gate,
    w_value,
    up_taps,
    up_bias,
    w_down,
):
    gate_full, value_full = in_one_piece((w_gate, w_value), "fs", 0, 1)
    whole = gathered_copies(tokens, "tp", 1)
    normed = rms_norm(whole, mix_gain)
    signal_full, outer_full, inner_full = in_one_piece(
        (w_signal, w_outer_gate, w_inner_gate), "fs", 0, 1
    )
    signal = jnp.dot(normed, signal_full, preferred_element_type=jnp.float32)
    outer = jnp.dot(normed, outer_full, preferred_element_type=jnp.float32)
    inner = jnp.dot(normed, inner_full, preferred_element_type=jnp.float32)
    signal = signal.astype(jnp.bfloat16).astype(jnp.float32)
    outer = outer.astype(jnp.bfloat16).astype(jnp.float32)
    inner = inner.astype(jnp.bfloat16).astype(jnp.float32)
    mixed = (outer * conv_positions(inner * signal, mix_taps)).astype(jnp.bfloat16)
    mix_terms = jnp.dot(
        mixed,
        lax.all_gather(w_mix_out, "fs", axis=1, tiled=True),
        preferred_element_type=jnp.float32,
    )
    mix_sum = sent_and_summed(mix_terms.astype(jnp.bfloat16), "tp", 1)
    resid = (tokens.astype(jnp.float32) + mix_sum).astype(jnp.bfloat16)
    whole_ffn = gathered_copies(resid, "tp", 1)
    normed_ffn = rms_norm(whole_ffn, ffn_gain)
    gate = jnp.dot(normed_ffn, gate_full, preferred_element_type=jnp.float32)
    value = jnp.dot(normed_ffn, value_full, preferred_element_type=jnp.float32)
    gate = gate.astype(jnp.bfloat16).astype(jnp.float32)
    value = value.astype(jnp.bfloat16).astype(jnp.float32)
    gate_conv = conv_positions(gate, up_taps[0]) + up_bias[0]
    value_conv = conv_positions(value, up_taps[1]) + up_bias[1]
    hidden = (jax.nn.silu(gate_conv) * value_conv).astype(jnp.bfloat16)
    ffn_terms = jnp.dot(
        hidden, lax.all_gather(w_down, "fs", axis=1, tiled=True), preferred_element_type=jnp.float32
    )
    ffn_sum = sent_and_summed(ffn_terms.astype(jnp.bfloat16), "tp", 1)
    return (resid.astype(jnp.float32) + ffn_sum).astype(jnp.bfloat16)


def solution(mesh):
    placed = (
        P(("grp", "fs"), "tp"),
        P(),
        P("fs", "tp"),
        P("fs", "tp"),
        P("fs", "tp"),
        P(None, "tp"),
        P("tp", "fs"),
        P(),
        P("fs", "tp"),
        P("fs", "tp"),
        P(None, None, "tp"),
        P(None, "tp"),
        P("tp", "fs"),
    )
    return jax.shard_map(
        on_device, mesh=mesh, in_specs=placed, out_specs=P(("grp", "fs"), "tp"), check_vma=False
    )
```

profile of v0, /device:TPU:40, one launch (start us, length us, event | category | flops | bytes accessed | tf_op | source)
XLA Modules:
  0.0 473.8 jit_solution(4301556435789790506)
XLA Ops:
  6.5 0.0 all-gather.4.cloned.1.call-start
  6.6 1.4 pad_maximum_fusion.1
  7.9 0.1 all-gather.4.cloned.1.call-update
  8.0 0.1 all-gather.6.cloned.1.call-start
  8.1 1.6 pad_maximum_fusion
  9.7 0.1 all-gather.6.cloned.1.call-update
  9.7 1.1 copy.16
  10.8 1.3 broadcast_in_dim.4
  12.1 0.0 copy-start.6
  12.1 0.0 copy-start.1
  12.1 4.7 all-to-all-start
  16.8 0.0 copy-done.6
  16.8 0.0 copy-start.3
  16.9 0.0 copy-done.1
  16.9 102.7 %all_gather.13 = bf16[128,2048]{0,1:T(8,128)(2,1)} all-gather(bf16[128,64]{0,1:T(8,128)(2,1)S(1)} %copy-done.1), channel_id=1, replica_groups=mesh['grp'=2,'fs'=32,'tp'=8] {'fs'}, dimensions={1}, use_global_device_ids=true | all-gather | bytes 540672 | tf_op jit(solution)/shard_map/all_gather | solution.py:93
  119.5 0.0 all-to-all-done
  119.5 0.4 multiply_reduce_fusion.1
  120.0 0.0 copy-done.3
  120.0 0.4 fusion.3
  120.4 48.9 %all-gather.4.cloned.1.call-done = bf16[2048,384]{1,0:T(8,128)(2,1)} async-done(((bf16[64,384]{1,0:T(8,128)(2,1)}), bf16[2048,384]{1,0:T(8,128)(2,1)}) %all-gather.4.cloned.1.call-update) | async-done | bytes 1572880 | tf_op jit(solution)/shard_map/all_gather | solution.py:12
  169.3 1.7 fusion.16
  170.9 1.7 fusion.15
  172.6 0.1 fusion.36
  172.7 3.0 convolution_convert_fusion.1
  175.7 1.3 copy.25
  177.0 4.4 all-to-all-start.1
  181.4 0.0 copy-start
  181.4 0.1 all-gather.8.cloned.1.call-start
  181.5 0.7 all-gather.8.cloned.1.call-update
  182.2 20.7 %all-to-all-done.1 = bf16[8,384,256]{2,1,0:T(8,128)(2,1)S(1)} async-done(((bf16[8,384,256]{2,1,0:T(8,128)(2,1)}), bf16[8,384,256]{2,1,0:T(8,128)(2,1)S(1)}, u32[]{:S(2)}, u32[]{:S(2)}) %all-to-all-start.1) | async-done | bytes 1572896 | tf_op jit(solution)/shard_map/all_to_all | solution.py:40
  202.9 0.2 convert_reduce_fusion.1
  203.2 0.0 copy-done
  203.2 0.1 add_convert_fusion.1
  203.2 0.2 copy.18
  203.4 1.4 broadcast_in_dim.5
  204.8 0.0 copy-start.5
  204.8 0.0 copy-start.2
  204.8 3.9 all-to-all-start.2
  208.7 0.0 copy-done.5
  208.7 0.0 copy-start.4
  208.7 0.0 copy-done.2
  208.8 21.2 %all-to-all-done.2 = bf16[8,384,256]{1,2,0:T(8,128)(2,1)S(1)} async-done(((bf16[8,384,256]{1,2,0:T(8,128)(2,1)}), bf16[8,384,256]{1,2,0:T(8,128)(2,1)S(1)}, u32[]{:S(2)}, u32[]{:S(2)}) %all-to-all-start.2) | async-done | bytes 1572896 | tf_op jit(solution)/shard_map/all_to_all | solution.py:18
  230.0 0.4 multiply_reduce_fusion
  230.5 0.0 copy-done.4
  230.5 0.4 fusion.1
  230.9 75.3 %all-gather.6.cloned.1.call-done = bf16[2048,1280]{1,0:T(8,128)(2,1)} async-done(((bf16[64,1280]{1,0:T(8,128)(2,1)}), bf16[2048,1280]{1,0:T(8,128)(2,1)}) %all-gather.6.cloned.1.call-update) | async-done | bytes 5242896 | tf_op jit(solution)/shard_map/all_gather | solution.py:12
  306.2 0.0 copy-start.7
  306.2 3.3 fusion.8
  309.5 0.1 convert.6
  309.6 0.0 copy-done.7
  309.6 1.4 fusion.11
  311.1 0.1 convert.7
  311.1 0.6 fusion.22
  311.7 0.3 fusion.29
  312.0 125.1 %all-gather.8.cloned.1.call-done = bf16[640,2048]{0,1:T(8,128)(2,1)} async-done(((bf16[640,64]{0,1:T(8,128)(2,1)}), bf16[640,2048]{0,1:T(8,128)(2,1)}) %all-gather.8.cloned.1.call-update) | async-done | bytes 2621456 | tf_op jit(solution)/shard_map/all_gather | solution.py:108
  437.2 3.2 convolution_convert_fusion
  440.3 0.1 copy.24
  440.4 25.8 %all_to_all.20 = bf16[8,384,256]{2,1,0:T(8,128)(2,1)S(1)} all-to-all(bf16[8,384,256]{2,1,0:T(8,128)(2,1)S(1)} %bitcast.61), channel_id=1, replica_groups=mesh['grp'=2,'fs'=32,'tp'=8] {'tp'}, dimensions={0} | all-to-all | bytes 3145728 | tf_op jit(solution)/shard_map/all_to_all | solution.py:40
  466.3 0.2 convert_reduce_fusion
  466.5 0.7 add_convert_fusion
  (5 shorter events, 0.1 us)
Async XLA Ops:
  6.5 162.7 %all-gather.4.cloned.1.call-start = ((), (), s32[]{:S(2)}) async-start(), calls=%async_computation.4 | async-start | bytes 1622016 | tf_op jit(solution)/shard_map/all_gather | solution.py:12
  8.0 298.2 %all-gather.6.cloned.1.call-start = ((), (), s32[]{:S(2)}) async-start(), calls=%async_computation.5 | async-start | bytes 5406720 | tf_op jit(solution)/shard_map/all_gather | solution.py:12
  12.1 4.7 copy-start.6
  12.1 4.8 %copy-start.1 = (bf16[128,64]{0,1:T(8,128)(2,1)S(1)}, bf16[128,64]{0,1:T(8,128)(2,1)}, u32[]{:S(2)}) copy-start(bf16[128,64]{0,1:T(8,128)(2,1)} %param.19) | copy-start | bytes 49156
  12.1 107.4 %all-to-all-start = ((bf16[8,384,256]{1,2,0:T(8,128)(2,1)}), bf16[8,384,256]{1,2,0:T(8,128)(2,1)S(1)}, u32[]{:S(2)}, u32[]{:S(2)}) async-start(bf16[8,384,256]{1,2,0:T(8,128)(2,1)} %broadcast_in_dim.4), calls=%async_computation | async-start | bytes 3145728 | tf_op jit(solution)/shard_map/all_to_all | solution.py:18
  16.8 103.1 %copy-start.3 = (f32[2048]{0:T(1024)S(1)}, f32[2048]{0:T(1024)}, u32[]{:S(2)}) copy-start(f32[2048]{0:T(1024)} %param.14) | copy-start | bytes 24580
  177.0 25.9 %all-to-all-start.1 = ((bf16[8,384,256]{2,1,0:T(8,128)(2,1)}), bf16[8,384,256]{2,1,0:T(8,128)(2,1)S(1)}, u32[]{:S(2)}, u32[]{:S(2)}) async-start(bf16[8,384,256]{2,1,0:T(8,128)(2,1)} %bitcast.59), calls=%async_computation.1 | async-start | bytes 3145728 | tf_op jit(solution)/shard_map/all_to_all | solution.py:40
  181.4 21.8 %copy-start = (bf16[384,256]{1,0:T(8,128)(2,1)S(1)}, bf16[384,256]{1,0:T(8,128)(2,1)}, u32[]{:S(2)}) copy-start(bf16[384,256]{1,0:T(8,128)(2,1)} %param.13) | copy-start | bytes 589828
  181.4 255.8 %all-gather.8.cloned.1.call-start = ((), (), s32[]{:S(2)}) async-start(), calls=%async_computation.6 | async-start | bytes 2703360 | tf_op jit(solution)/shard_map/all_gather | solution.py:108
  204.8 3.9 copy-start.5
  204.8 4.0 copy-start.2
  204.8 25.3 %all-to-all-start.2 = ((bf16[8,384,256]{1,2,0:T(8,128)(2,1)}), bf16[8,384,256]{1,2,0:T(8,128)(2,1)S(1)}, u32[]{:S(2)}, u32[]{:S(2)}) async-start(bf16[8,384,256]{1,2,0:T(8,128)(2,1)} %broadcast_in_dim.5), calls=%async_computation.2 | async-start | bytes 3145728 | tf_op jit(solution)/shard_map/all_to_all | solution.py:18
  208.7 21.8 %copy-start.4 = (f32[2048]{0:T(1024)S(1)}, f32[2048]{0:T(1024)}, u32[]{:S(2)}) copy-start(f32[2048]{0:T(1024)} %param.20) | copy-start | bytes 24580
  306.2 3.4 copy-start.7
Sparse Core Ops, SparseCore 0:
  9.4 159.7 all-gather.3
  171.4 134.7 all-gather.5
  308.3 128.8 all-gather.7
where the time goes:
time: 475 us; the launch traced here: 474 us
  waiting for transfers between devices  292 us (61%)
  blocking collectives  129 us (27%)
  matrix products  14.3 us (3%)
  between operations  13.3 us (3%)
  starting transfers between devices  13.1 us (3%)
  other arithmetic  6.94 us (1%)
  local copies, waits for them, and re-layouts  5.45 us (1%)
    all_gather x1, waiting for transfers between devices, on_device(): lax.all_gather(w_down, 'fs', axis=1, tiled=True)  125 us
    all_gather x2, waiting for transfers between devices, in_one_piece(): filled = lax.all_gather(both, axis, axis=dim, tiled=True)  124 us
    all_gather x1, blocking collectives, on_device(): lax.all_gather(w_mix_out, 'fs', axis=1, tiled=True)  103 us
    all_to_all x1, blocking collectives, sent_and_summed(): lax.all_to_all(split_up(value, dim, devices), axis, 0, 0, tiled=True)  25.8 us
    all_to_all x2, waiting for transfers between devices, copy_for_each(): return lax.all_to_all(copies, axis, split_axis=0, concat_axis=0, tiled=True)  21.2 us
    all_to_all x1, waiting for transfers between devices, sent_and_summed(): lax.all_to_all(split_up(value, dim, devices), axis, 0, 0, tiled=True)  20.7 us
  transfers between devices with their start and end apart: 6, of which 5 were waited for; matrix products, arithmetic and copies ran while one was open for 4% of the time, Pallas kernels for 0%

commit v1 on v0

--- a/solution.py
+++ b/solution.py
@@ -60,6 +60,12 @@
     return (values * scale * gain).astype(jnp.bfloat16)
 
 
+def dot_t(left, right_t):
+    return lax.dot_general(
+        left, right_t, (((1,), (1,)), ((), ())), preferred_element_type=jnp.float32
+    )
+
+
 def on_device(
     tokens,
     mix_gain,
@@ -75,12 +81,18 @@
     up_bias,
     w_down,
 ):
-    gate_full, value_full = in_one_piece((w_gate, w_value), "fs", 0, 1)
+    shards = (w_signal, w_outer_gate, w_inner_gate, w_mix_out.T, w_gate, w_value, w_down.T)
+    (
+        signal_full,
+        outer_full,
+        inner_full,
+        mix_out_t,
+        gate_full,
+        value_full,
+        down_t,
+    ) = in_one_piece(shards, "fs", 0, 1)
     whole = gathered_copies(tokens, "tp", 1)
     normed = rms_norm(whole, mix_gain)
-    signal_full, outer_full, inner_full = in_one_piece(
-        (w_signal, w_outer_gate, w_inner_gate), "fs", 0, 1
-    )
     signal = jnp.dot(normed, signal_full, preferred_element_type=jnp.float32)
     outer = jnp.dot(normed, outer_full, preferred_element_type=jnp.float32)
     inner = jnp.dot(normed, inner_full, preferred_element_type=jnp.float32)
@@ -88,11 +100,7 @@
     outer = outer.astype(jnp.bfloat16).astype(jnp.float32)
     inner = inner.astype(jnp.bfloat16).astype(jnp.float32)
     mixed = (outer * conv_positions(inner * signal, mix_taps)).astype(jnp.bfloat16)
-    mix_terms = jnp.dot(
-        mixed,
-        lax.all_gather(w_mix_out, "fs", axis=1, tiled=True),
-        preferred_element_type=jnp.float32,
-    )
+    mix_terms = dot_t(mixed, mix_out_t)
     mix_sum = sent_and_summed(mix_terms.astype(jnp.bfloat16), "tp", 1)
     resid = (tokens.astype(jnp.float32) + mix_sum).astype(jnp.bfloat16)
     whole_ffn = gathered_copies(resid, "tp", 1)
@@ -104,9 +112,7 @@
     gate_conv = conv_positions(gate, up_taps[0]) + up_bias[0]
     value_conv = conv_positions(value, up_taps[1]) + up_bias[1]
     hidden = (jax.nn.silu(gate_conv) * value_conv).astype(jnp.bfloat16)
-    ffn_terms = jnp.dot(
-        hidden, lax.all_gather(w_down, "fs", axis=1, tiled=True), preferred_element_type=jnp.float32
-    )
+    ffn_terms = dot_t(hidden, down_t)
     ffn_sum = sent_and_summed(ffn_terms.astype(jnp.bfloat16), "tp", 1)
     return (resid.astype(jnp.float32) + ffn_sum).astype(jnp.bfloat16)
 

time: 475 us -> 296 us (0.62)
  waiting for transfers between devices: 292 us -> 191 us
  blocking collectives: 129 us -> 50.2 us
  local copies, waits for them, and re-layouts: 5.45 us -> 10.5 us
    all_gather x1 -> x0, waiting for transfers between devices: 125 us -> none  [on_device(): lax.all_gather(w_down, 'fs', axis=1, tiled=True)]
    all_gather x1 -> x0, blocking collectives: 103 us -> none  [on_device(): lax.all_gather(w_mix_out, 'fs', axis=1, tiled=True)]
    all_to_all x1 -> x2, blocking collectives: 25.8 us -> 50.2 us  [sent_and_summed(): lax.all_to_all(split_up(value, dim, devices), axis, 0, 0, tiled=True)]
    all_gather x2 -> x1, waiting for transfers between devices: 124 us -> 148 us  [in_one_piece(): filled = lax.all_gather(both, axis, axis=dim, tiled=True)]
    all_to_all x2, waiting for transfers between devices: 21.2 us -> 42.8 us  [copy_for_each(): return lax.all_to_all(copies, axis, split_axis=0, concat_axis=0, tiled=True)]
    all_to_all x1 -> x0, waiting for transfers between devices: 20.7 us -> none  [sent_and_summed(): lax.all_to_all(split_up(value, dim, devices), axis, 0, 0, tiled=True)]
    unnamed x17 -> x21, local copies, waits for them, and re-layouts: 1.13 us -> 6.54 us
  transfers between devices with their start and end apart: 6 -> 3, of which waited for: 5 -> 3; matrix products, arithmetic and copies ran while one was open for 4% -> 1% of each run, Pallas kernels for 0% -> 0%
where the time goes in v1:
time: 296 us; the launch traced here: 294 us
  waiting for transfers between devices  191 us (65%)
  blocking collectives  50.2 us (17%)
  matrix products  15.9 us (5%)
  between operations  13.6 us (5%)
  local copies, waits for them, and re-layouts  10.5 us (4%)
  starting transfers between devices  8.64 us (3%)
  other arithmetic  3.95 us (1%)
    all_gather x1, waiting for transfers between devices, in_one_piece(): filled = lax.all_gather(both, axis, axis=dim, tiled=True)  148 us
    all_to_all x2, blocking collectives, sent_and_summed(): lax.all_to_all(split_up(value, dim, devices), axis, 0, 0, tiled=True)  50.2 us
    all_to_all x2, waiting for transfers between devices, copy_for_each(): return lax.all_to_all(copies, axis, split_axis=0, concat_axis=0, tiled=True)  42.8 us
    all_to_all x2, starting transfers between devices, copy_for_each(): return lax.all_to_all(copies, axis, split_axis=0, concat_axis=0, tiled=True)  8.63 us
    unnamed x21, local copies, waits for them, and re-layouts  6.54 us
    dot_general x2, matrix products, dot_t(): lax.dot_general(left, right_t, (((1,), (1,)), ((), ())), preferred_elemen...  6.23 us
  transfers between devices with their start and end apart: 3, of which 3 were waited for; matrix products, arithmetic and copies ran while one was open for 1% of the time, Pallas kernels for 0%

profile of v1, /device:TPU:40, one launch (start us, length us, event | category | flops | bytes accessed | tf_op | source)
XLA Modules:
  0.0 294.1 jit_solution(14965353285934270448)
XLA Ops:
  6.5 0.0 all-gather.2.cloned.1.call-start
  6.6 0.7 constant_dynamic-update-slice_fusion.5
  7.3 0.7 constant_dynamic-update-slice_fusion.4
  8.0 0.7 constant_dynamic-update-slice_fusion.3
  8.7 0.7 constant_dynamic-update-slice_fusion.2
  9.4 0.9 constant_dynamic-update-slice_fusion.1
  10.4 0.9 constant_dynamic-update-slice_fusion
  11.3 0.9 bitcast_dynamic-update-slice_fusion
  12.2 0.0 copy-start.1
  12.2 0.7 copy-done.1
  12.9 0.1 all-gather.2.cloned.1.call-update
  12.9 0.0 copy-start.6
  13.0 1.1 copy.16
  14.0 1.3 broadcast_in_dim.4
  15.3 0.0 copy-start.3
  15.3 4.7 %all-to-all-start = ((bf16[8,384,256]{1,2,0:T(8,128)(2,1)}), bf16[8,384,256]{1,2,0:T(8,128)(2,1)S(1)}, u32[]{:S(2)}, u32[]{:S(2)}) async-start(bf16[8,384,256]{1,2,0:T(8,128)(2,1)} %broadcast_in_dim.4), calls=%async_computation | async-start | bytes 3145728 | tf_op jit(solution)/shard_map/all_to_all | solution.py:18
  20.1 0.0 copy-done.6
  20.1 21.5 %all-to-all-done = bf16[8,384,256]{1,2,0:T(8,128)(2,1)S(1)} async-done(((bf16[8,384,256]{1,2,0:T(8,128)(2,1)}), bf16[8,384,256]{1,2,0:T(8,128)(2,1)S(1)}, u32[]{:S(2)}, u32[]{:S(2)}) %all-to-all-start) | async-done | bytes 1572896 | tf_op jit(solution)/shard_map/all_to_all | solution.py:18
  41.6 0.4 multiply_reduce_fusion.1
  42.0 0.0 copy-done.3
  42.0 0.4 fusion.3
  42.5 148.5 %all-gather.2.cloned.1.call-done = bf16[2048,2432]{1,0:T(8,128)(2,1)} async-done(((bf16[64,2432]{1,0:T(8,128)(2,1)}), bf16[2048,2432]{1,0:T(8,128)(2,1)}) %all-gather.2.cloned.1.call-update) | async-done | bytes 9961488 | tf_op jit(solution)/shard_map/all_gather | solution.py:12
  190.9 1.6 fusion.17
  192.6 1.6 fusion.16
  194.2 0.1 fusion.38
  194.3 3.0 %convolution_convert_fusion.1 = bf16[384,2048]{1,0:T(8,128)(2,1)S(1)} fusion(f32[384,128]{1,0:T(8,128)S(1)} %bitcast.67, bf16[384,2048]{0,1:T(8,128)(2,1)S(1)} %fusion.3, bf16[2048,2432]{1,0:T(8,128)(2,1)} %all-gather.2.cloned.1.call-done), kind=kOutput, calls=%fused_computation.11 | convolution fusion | flops 403636224 | bytes 4390912 | tf_op jit(solution)/shard_map/dot_general | solution.py:64
  197.3 0.1 copy.25
  197.4 0.0 copy-start
  197.5 26.0 %all_to_all.20 = bf16[8,384,256]{2,1,0:T(8,128)(2,1)S(1)} all-to-all(bf16[8,384,256]{2,1,0:T(8,128)(2,1)S(1)} %bitcast.63), channel_id=1, replica_groups=mesh['grp'=2,'fs'=32,'tp'=8] {'tp'}, dimensions={0} | all-to-all | bytes 3145728 | tf_op jit(solution)/shard_map/all_to_all | solution.py:40
  223.5 0.2 convert_reduce_fusion.1
  223.7 0.0 copy-done
  223.7 0.1 add_convert_fusion.1
  223.8 0.0 copy-start.5
  223.8 0.0 copy-start.2
  223.8 0.2 copy.18
  224.0 1.3 broadcast_in_dim.5
  225.3 0.0 copy-start.4
  225.3 3.9 %all-to-all-start.2 = ((bf16[8,384,256]{1,2,0:T(8,128)(2,1)}), bf16[8,384,256]{1,2,0:T(8,128)(2,1)S(1)}, u32[]{:S(2)}, u32[]{:S(2)}) async-start(bf16[8,384,256]{1,2,0:T(8,128)(2,1)} %broadcast_in_dim.5), calls=%async_computation.2 | async-start | bytes 3145728 | tf_op jit(solution)/shard_map/all_to_all | solution.py:18
  229.2 0.0 copy-done.5
  229.2 0.0 copy-done.2
  229.3 21.2 %all-to-all-done.2 = bf16[8,384,256]{1,2,0:T(8,128)(2,1)S(1)} async-done(((bf16[8,384,256]{1,2,0:T(8,128)(2,1)}), bf16[8,384,256]{1,2,0:T(8,128)(2,1)S(1)}, u32[]{:S(2)}, u32[]{:S(2)}) %all-to-all-start.2) | async-done | bytes 1572896 | tf_op jit(solution)/shard_map/all_to_all | solution.py:18
  250.5 0.4 multiply_reduce_fusion
  251.0 0.0 copy-done.4
  251.0 0.4 fusion.1
  251.4 3.2 %fusion.12 = bf16[384,640]{1,0:T(8,128)(2,1)S(1)} fusion(bf16[384,2048]{0,1:T(8,128)(2,1)S(1)} %fusion.1, bf16[2048,2432]{1,0:T(8,128)(2,1)} %all-gather.2.cloned.1.call-done), kind=kOutput, calls=%fused_computation.20 | convolution fusion | flops 1006878720 | bytes 4685824 | tf_op jit(solution)/shard_map/dot_general | solution.py:109
  254.6 0.1 convert.7
  254.7 3.2 %fusion.9 = bf16[384,640]{1,0:T(8,128)(2,1)S(1)} fusion(bf16[384,2048]{0,1:T(8,128)(2,1)S(1)} %fusion.1, bf16[2048,2432]{1,0:T(8,128)(2,1)} %all-gather.2.cloned.1.call-done), kind=kOutput, calls=%fused_computation.19 | convolution fusion | flops 1006878720 | bytes 4685824 | tf_op jit(solution)/shard_map/dot_general | solution.py:108
  257.9 0.1 convert.6
  257.9 0.6 fusion.23
  258.5 0.3 fusion.30
  258.8 3.2 %convolution_convert_fusion = bf16[384,2048]{1,0:T(8,128)(2,1)S(1)} fusion(bf16[384,640]{1,0:T(8,128)(2,1)S(1)} %fusion.30, bf16[2048,2432]{1,0:T(8,128)(2,1)} %all-gather.2.cloned.1.call-done), kind=kOutput, calls=%fused_computation.10 | convolution fusion | flops 1007419392 | bytes 4685824 | tf_op jit(solution)/shard_map/dot_general | solution.py:64
  262.0 0.1 copy.24
  262.1 24.1 %all_to_all.21 = bf16[8,384,256]{2,1,0:T(8,128)(2,1)S(1)} all-to-all(bf16[8,384,256]{2,1,0:T(8,128)(2,1)S(1)} %bitcast.64), channel_id=1, replica_groups=mesh['grp'=2,'fs'=32,'tp'=8] {'tp'}, dimensions={0} | all-to-all | bytes 3145728 | tf_op jit(solution)/shard_map/all_to_all | solution.py:40
  286.2 0.2 convert_reduce_fusion
  286.5 0.7 add_convert_fusion
  (5 shorter events, 0.1 us)
Async XLA Ops:
  6.5 184.4 %all-gather.2.cloned.1.call-start = ((), (), s32[]{:S(2)}) async-start(), calls=%async_computation.4 | async-start | bytes 10272768 | tf_op jit(solution)/shard_map/all_gather | solution.py:12
  12.2 0.7 copy-start.1
  12.9 7.1 %copy-start.6 = (f32[3,128]{1,0:T(4,128)S(1)}, f32[3,128]{1,0:T(4,128)}, u32[]{:S(2)}) copy-start(f32[3,128]{1,0:T(4,128)} %param.18) | copy-start | bytes 4612
  15.3 26.7 %copy-start.3 = (f32[2048]{0:T(1024)S(1)}, f32[2048]{0:T(1024)}, u32[]{:S(2)}) copy-start(f32[2048]{0:T(1024)} %param.14) | copy-start | bytes 24580
  15.3 26.3 %all-to-all-start = ((bf16[8,384,256]{1,2,0:T(8,128)(2,1)}), bf16[8,384,256]{1,2,0:T(8,128)(2,1)S(1)}, u32[]{:S(2)}, u32[]{:S(2)}) async-start(bf16[8,384,256]{1,2,0:T(8,128)(2,1)} %broadcast_in_dim.4), calls=%async_computation | async-start | bytes 3145728 | tf_op jit(solution)/shard_map/all_to_all | solution.py:18
  197.4 26.3 %copy-start = (bf16[384,256]{1,0:T(8,128)(2,1)S(1)}, bf16[384,256]{1,0:T(8,128)(2,1)}, u32[]{:S(2)}) copy-start(bf16[384,256]{1,0:T(8,128)(2,1)} %param.13) | copy-start | bytes 589828
  223.8 5.4 %copy-start.5 = (f32[2,640]{1,0:T(2,128)S(1)}, f32[2,640]{1,0:T(2,128)}, u32[]{:S(2)}) copy-start(f32[2,640]{1,0:T(2,128)} %param.24) | copy-start | bytes 15364
  223.8 5.4 %copy-start.2 = (f32[2,3,640]{2,0,1:T(2,128)S(1)}, f32[2,3,640]{2,0,1:T(2,128)}, u32[]{:S(2)}) copy-start(f32[2,3,640]{2,0,1:T(2,128)} %param.23) | copy-start | bytes 46084
  225.3 25.7 %copy-start.4 = (f32[2048]{0:T(1024)S(1)}, f32[2048]{0:T(1024)}, u32[]{:S(2)}) copy-start(f32[2048]{0:T(1024)} %param.20) | copy-start | bytes 24580
  225.3 25.3 %all-to-all-start.2 = ((bf16[8,384,256]{1,2,0:T(8,128)(2,1)}), bf16[8,384,256]{1,2,0:T(8,128)(2,1)S(1)}, u32[]{:S(2)}, u32[]{:S(2)}) async-start(bf16[8,384,256]{1,2,0:T(8,128)(2,1)} %broadcast_in_dim.5), calls=%async_computation.2 | async-start | bytes 3145728 | tf_op jit(solution)/shard_map/all_to_all | solution.py:18
Sparse Core Ops, SparseCore 0:
  13.1 177.8 all-gather.1

commit v2 on v1

v2 whole, which is shorter than its diff:
```python
import jax
import jax.numpy as jnp
from jax import lax
from jax.sharding import Mesh
from jax.sharding import PartitionSpec as P

SEQS_DEV = 2
CORES = 2
NEAR = 4

TP = ("tx", "tc")
FS = ("fa", "fb")


def side_by_side(arrays):
    return jnp.concatenate(arrays, axis=1)


def gathered_copies(value, axis):
    count = lax.axis_size(axis)
    copies = jnp.broadcast_to(value, (count, *value.shape))
    pieces = lax.all_to_all(copies, axis, split_axis=0, concat_axis=0, tiled=True)
    rows, width = value.shape
    return jnp.moveaxis(pieces, 0, 1).reshape(rows, count * width)


def swapped(value, axis):
    return lax.ppermute(value, axis, [(0, 1), (1, 0)])


def by_core(own, other):
    first = lax.axis_index("tc") == 0
    return jnp.where(first, own, other), jnp.where(first, other, own)


def gathered_features(value):
    own = lax.all_gather(value, "tx", axis=0)
    other = swapped(own, "tc")
    pieces = [piece for chip in range(own.shape[0]) for piece in by_core(own[chip], other[chip])]
    return jnp.concatenate(pieces, axis=1)


def sent_and_summed(terms):
    chips = lax.axis_size("tx")
    width = terms.shape[1] // (chips * CORES)
    blocks = [terms[:, k * width : (k + 1) * width] for k in range(chips * CORES)]
    chosen = [by_core(*blocks[k : k + CORES]) for k in range(0, chips * CORES, CORES)]
    keep = jnp.stack([pair[0] for pair in chosen])
    send = jnp.stack([pair[1] for pair in chosen])
    received = swapped(send.astype(jnp.bfloat16), "tc")
    pairs = (keep + received.astype(jnp.float32)).astype(jnp.bfloat16)
    parts = lax.all_to_all(pairs, "tx", 0, 0, tiled=True)
    return jnp.sum(parts.astype(jnp.float32), axis=0)


def conv_positions(values, taps):
    width = values.shape[1]
    blocks = values.reshape(SEQS_DEV, -1, width)
    length = blocks.shape[1]
    padded = jnp.pad(blocks, ((0, 0), (2, 0), (0, 0)))
    result = (
        padded[:, 0:length] * taps[0]
        + padded[:, 1 : length + 1] * taps[1]
        + padded[:, 2 : length + 2] * taps[2]
    )
    return result.reshape(-1, width)


def rms_norm(stream, gain):
    values = stream.astype(jnp.float32)
    scale = lax.rsqrt(jnp.mean(values * values, axis=-1, keepdims=True) + 1e-06)
    return (values * scale * gain).astype(jnp.bfloat16)


def dot(left, right):
    return jnp.dot(left, right, preferred_element_type=jnp.float32)


def dot_t(left, right_t):
    return lax.dot_general(
        left, right_t, (((1,), (1,)), ((), ())), preferred_element_type=jnp.float32
    )


def near_gather(far):
    wide = lax.all_gather(far, "fb", axis=1, tiled=True)
    return wide.reshape(-1, far.shape[-1])


def rounded(value):
    return value.astype(jnp.bfloat16).astype(jnp.float32)


def mixer_weights(w_signal, w_outer_gate, w_inner_gate, mix_out_t, paired):
    if not paired:
        shards = (w_signal, w_inner_gate, w_outer_gate, mix_out_t)
        far = lax.all_gather(side_by_side(shards), "fa", axis=0)
        width = w_signal.shape[1]
        return tuple(near_gather(far[:, :, k * width : (k + 1) * width]) for k in range(4))
    first = lax.axis_index("pair") == 0
    early = jnp.where(first, w_signal, w_inner_gate)
    late = jnp.where(first, w_outer_gate, mix_out_t)
    width = early.shape[1]
    far = lax.all_gather(side_by_side((early, late)), "fa", axis=0)
    early_own = near_gather(far[:, :, :width])
    early_other = swapped(early_own, "pair")
    late_own = near_gather(far[:, :, width:])
    late_other = swapped(late_own, "pair")
    outer_full = jnp.where(first, late_own, late_other)
    mix_full = jnp.where(first, late_other, late_own)
    return early_own, early_other, outer_full, mix_full


def on_device(
    tokens,
    mix_gain,
    w_signal,
    w_outer_gate,
    w_inner_gate,
    mix_taps,
    w_mix_out,
    ffn_gain,
    w_gate,
    w_value,
    up_taps,
    up_bias,
    w_down,
    paired,
):
    hidden_width = w_gate.shape[1]
    ffn_full = lax.all_gather(side_by_side((w_gate, w_value, w_down.T)), FS, axis=0, tiled=True)
    whole = gathered_copies(tokens, TP)
    early_a, early_b, outer_full, mix_full = mixer_weights(
        w_signal, w_outer_gate, w_inner_gate, w_mix_out.T, paired
    )
    normed = rms_norm(whole, mix_gain)
    product = rounded(dot(normed, early_a)) * rounded(dot(normed, early_b))
    outer = rounded(dot(normed, outer_full))
    mixed = (outer * conv_positions(product, mix_taps)).astype(jnp.bfloat16)
    mix_sum = sent_and_summed(dot_t(mixed, mix_full))
    resid = (tokens.astype(jnp.float32) + mix_sum).astype(jnp.bfloat16)
    whole_ffn = gathered_features(resid)
    normed_ffn = rms_norm(whole_ffn, ffn_gain)
    gate = rounded(dot(normed_ffn, ffn_full[:, :hidden_width]))
    value = rounded(dot(normed_ffn, ffn_full[:, hidden_width : 2 * hidden_width]))
    gate_conv = conv_positions(gate, up_taps[0]) + up_bias[0]
    value_conv = conv_positions(value, up_taps[1]) + up_bias[1]
    hidden = (jax.nn.silu(gate_conv) * value_conv).astype(jnp.bfloat16)
    ffn_sum = sent_and_summed(dot_t(hidden, ffn_full[:, 2 * hidden_width :]))
    return (resid.astype(jnp.float32) + ffn_sum).astype(jnp.bfloat16)


def solution(mesh):
    groups, depth, wide = (mesh.shape[name] for name in ("grp", "fs", "tp"))
    pair = 2 if groups % 2 == 0 else 1
    split = Mesh(
        mesh.devices.reshape(
            groups // pair, pair, depth // NEAR, NEAR, wide // CORES, CORES
        ),
        ("gp", "pair", *FS, *TP),
    )
    streams = P(("gp", "pair", *FS), TP)
    placed = (
        streams,
        P(),
        P(FS, TP),
        P(FS, TP),
        P(FS, TP),
        P(None, TP),
        P(TP, FS),
        P(),
        P(FS, TP),
        P(FS, TP),
        P(None, None, TP),
        P(None, TP),
        P(TP, FS),
    )

    def body(*args):
        return on_device(*args, paired=pair == 2)

    return jax.shard_map(
        body, mesh=split, in_specs=placed, out_specs=streams, check_vma=False
    )
```

time: 296 us -> 233 us (0.79)
  waiting for transfers between devices: 191 us -> 11.8 us
  blocking collectives: 50.2 us -> 167 us
  starting transfers between devices: 8.64 us -> 16.2 us
  local copies, waits for them, and re-layouts: 10.5 us -> 4.25 us
  matrix products: 15.9 us -> 12.4 us
    all_gather x1, waiting for transfers between devices: 148 us -> 2.02 us  [on_device(): lax.all_gather(side_by_side((w_gate, w_value, w_down.T)), FS, axis=0, til...]
    all_gather x0 -> x4, blocking collectives: none -> 133 us  [the longest x1 74.1 us: mixer_weights(): far = lax.all_gather(side_by_side((early, late)), 'fa', axis=0)]
    all_to_all x2 -> x1, waiting for transfers between devices: 42.8 us -> 0.01 us  [gathered_copies(): lax.all_to_all(copies, axis, split_axis=0, concat_axis=0, tiled=True)]
    all_to_all x2, blocking collectives: 50.2 us -> 33.4 us  [sent_and_summed(): parts = lax.all_to_all(pairs, 'tx', 0, 0, tiled=True)]
    ppermute x0 -> x5, starting transfers between devices: none -> 11.5 us  [swapped(): return lax.ppermute(value, axis, [(0, 1), (1, 0)])]
    ppermute x0 -> x5, waiting for transfers between devices: none -> 9.74 us  [swapped(): return lax.ppermute(value, axis, [(0, 1), (1, 0)])]
    all_to_all x2 -> x1, starting transfers between devices: 8.63 us -> 4.73 us  [gathered_copies(): lax.all_to_all(copies, axis, split_axis=0, concat_axis=0, tiled=True)]
    unnamed x21 -> x29, local copies, waits for them, and re-layouts: 6.54 us -> 2.74 us
  transfers between devices with their start and end apart: 3 -> 7, of which waited for: 3 -> 5; matrix products, arithmetic and copies ran while one was open for 1% -> 5% of each run, Pallas kernels for 0% -> 0%
where the time goes in v2:
time: 233 us; the launch traced here: 232 us
  blocking collectives  167 us (72%)
  starting transfers between devices  16.2 us (7%)
  between operations  13.8 us (6%)
  matrix products  12.4 us (5%)
  waiting for transfers between devices  11.8 us (5%)
  other arithmetic  6.75 us (3%)
  local copies, waits for them, and re-layouts  4.25 us (2%)
    all_gather x1, blocking collectives, mixer_weights(): far = lax.all_gather(side_by_side((early, late)), 'fa', axis=0)  74.1 us
    all_gather x2, blocking collectives, near_gather(): wide = lax.all_gather(far, 'fb', axis=1, tiled=True)  44.9 us
    all_to_all x2, blocking collectives, sent_and_summed(): parts = lax.all_to_all(pairs, 'tx', 0, 0, tiled=True)  33.4 us
    all_gather x1, blocking collectives, gathered_features(): own = lax.all_gather(value, 'tx', axis=0)  14.4 us
    ppermute x5, starting transfers between devices, swapped(): return lax.ppermute(value, axis, [(0, 1), (1, 0)])  11.5 us
    ppermute x5, waiting for transfers between devices, swapped(): return lax.ppermute(value, axis, [(0, 1), (1, 0)])  9.74 us
    dot_general x4, matrix products, dot(): return jnp.dot(left, right, preferred_element_type=jnp.float32)  7.48 us
    dot_general x2, matrix products, dot_t(): lax.dot_general(left, right_t, (((1,), (1,)), ((), ())), preferred_elemen...  4.92 us
  transfers between devices with their start and end apart: 7, of which 5 were waited for; matrix products, arithmetic and copies ran while one was open for 5% of the time, Pallas kernels for 0%

profile of v2, /device:TPU:40, one launch (start us, length us, event | category | flops | bytes accessed | tf_op | source)
XLA Modules:
  0.0 232.0 jit_solution(11282291120822975202)
XLA Ops:
  6.6 1.7 pad_maximum_fusion.2
  8.2 0.1 all-gather.4.cloned.1.call-update
  8.3 1.1 copy.14
  9.4 1.4 broadcast_in_dim.2
  10.8 4.7 %all-to-all-start = ((bf16[8,384,256]{1,2,0:T(8,128)(2,1)}), bf16[8,384,256]{1,2,0:T(8,128)(2,1)S(1)}, u32[]{:S(2)}, u32[]{:S(2)}) async-start(bf16[8,384,256]{1,2,0:T(8,128)(2,1)} %broadcast_in_dim.2), calls=%async_computation | async-start | bytes 3145728 | tf_op jit(solution)/shard_map/all_to_all | solution.py:22
  15.5 0.0 copy-start.11
  15.6 74.1 %all-gather = bf16[512,256]{1,0:T(8,128)(2,1)S(1)} all-gather(bf16[64,256]{1,0:T(8,128)(2,1)S(1)} %pad_maximum_fusion.3), channel_id=2, replica_groups=mesh['gp'=1,'pair'=2,'fa'=8,'fb'=4,'tx'=4,'tc'=2] {'fa'}, dimensions={0}, use_global_device_ids=true | all-gather | bytes 294912 | tf_op jit(solution)/shard_map/all_gather | solution.py:104
  89.7 0.1 fusion.69
  89.7 24.0 %all_gather.24 = bf16[8,256,128]{2,1,0:T(8,128)(2,1)S(1)} all-gather(bf16[8,64,128]{2,1,0:T(8,128)(2,1)S(1)} %get-tuple-element.30), channel_id=1, replica_groups=mesh['gp'=1,'pair'=2,'fa'=8,'fb'=4,'tx'=4,'tc'=2] {'fb'}, dimensions={1}, use_global_device_ids=true | all-gather | bytes 655360 | tf_op jit(solution)/shard_map/all_gather | solution.py:86
  113.7 1.9 collective-permute-start.1
  115.7 20.9 %all_gather.23 = bf16[8,256,128]{2,1,0:T(8,128)(2,1)S(1)} all-gather(bf16[8,64,128]{2,1,0:T(8,128)(2,1)S(1)} %get-tuple-element.29), channel_id=1, replica_groups=mesh['gp'=1,'pair'=2,'fa'=8,'fb'=4,'tx'=4,'tc'=2] {'fb'}, dimensions={1}, use_global_device_ids=true | all-gather | bytes 655360 | tf_op jit(solution)/shard_map/all_gather | solution.py:86
  136.6 3.5 %collective-permute-start = (bf16[2048,128]{1,0:T(8,128)(2,1)S(1)}, bf16[2048,128]{1,0:T(8,128)(2,1)S(1)}, u32[]{:S(2)}, u32[]{:S(2)}) collective-permute-start(bf16[2048,128]{1,0:T(8,128)(2,1)S(1)} %bitcast.130), channel_id=1, source_target_pairs={{0,256},{256,0},{1,257},{257,1},{2,258},{258,2},{3,259},{259,3},{4... | collective-permute-start | bytes 1572872 | tf_op jit(solution)/shard_map/ppermute | solution.py:28
  140.2 0.0 all-to-all-done
  140.2 0.4 multiply_reduce_fusion
  140.6 0.4 fusion.4
  141.1 1.0 fusion.31
  142.1 0.0 collective-permute-done.1
  142.1 0.2 copy-done
  142.3 1.7 fusion.35
  143.9 0.1 fusion.59
  144.0 3.7 %collective-permute-done = bf16[2048,128]{1,0:T(8,128)(2,1)S(1)} collective-permute-done((bf16[2048,128]{1,0:T(8,128)(2,1)S(1)}, bf16[2048,128]{1,0:T(8,128)(2,1)S(1)}, u32[]{:S(2)}, u32[]{:S(2)}) %collective-permute-start) | collective-permute-done | bytes 524320 | tf_op jit(solution)/shard_map/ppermute | solution.py:28
  147.7 0.8 copy-done.2
  148.5 3.5 %fusion.39 = f32[384,2048]{1,0:T(8,128)S(1)} fusion(f32[384,128]{1,0:T(8,128)S(1)} %bitcast.134, bf16[384,2048]{0,1:T(8,128)(2,1)} %copy-done, bf16[2048,128]{1,0:T(8,128)(2,1)} %copy-done.2, bf16[2048,128]{1,0:T(8,128)(2,1)} %bitcast.131, pred[]{:T(512)S(6)} %eq.5), kind=kOutput, calls=%fused_computation.39 | convolution fusion | flops 403374080 | bytes 5963777 | tf_op jit(solution)/shard_map/dot_general | solution.py:80
  152.0 0.1 fusion.61
  152.1 0.1 pad_maximum_fusion
  152.3 2.0 collective-permute-start.2
  154.2 0.2 select_bitcast_fusion.7
  154.4 2.0 collective-permute-done.2
  156.5 0.2 fusion.14
  156.7 0.0 copy-start.3
  156.7 17.0 %all_to_all.15 = bf16[4,384,256]{2,1,0:T(8,128)(2,1)S(1)} all-to-all(bf16[4,384,256]{2,1,0:T(8,128)(2,1)S(1)} %fusion.14), channel_id=1, replica_groups=mesh['gp'=1,'pair'=2,'fa'=8,'fb'=4,'tx'=4,'tc'=2] {'tx'}, dimensions={0} | all-to-all | bytes 1572864 | tf_op jit(solution)/shard_map/all_to_all | solution.py:52
  173.7 0.1 convert_reduce_fusion.1
  173.8 14.4 %all-gather.1 = bf16[1536,256]{1,0:T(8,128)(2,1)S(1)} all-gather(bf16[384,256]{1,0:T(8,128)(2,1)S(1)} %add_convert_fusion.1), channel_id=3, replica_groups=mesh['gp'=1,'pair'=2,'fa'=8,'fb'=4,'tx'=4,'tc'=2] {'tx'}, dimensions={0}, use_global_device_ids=true | all-gather | bytes 983040 | tf_op jit(solution)/shard_map/all_gather | solution.py:37
  188.2 2.1 collective-permute-start.3
  190.5 2.0 collective-permute-done.3
  192.4 0.1 bitcast_dynamic-update-slice_fusion.7
  192.5 0.1 bitcast_dynamic-update-slice_fusion.6
  192.5 0.1 bitcast_dynamic-update-slice_fusion.5
  192.6 0.1 bitcast_dynamic-update-slice_fusion.4
  192.7 0.1 bitcast_dynamic-update-slice_fusion.3
  192.7 0.0 copy-start.13
  192.7 0.1 bitcast_dynamic-update-slice_fusion.2
  192.8 0.1 bitcast_dynamic-update-slice_fusion.1
  192.9 0.1 bitcast_dynamic-update-slice_fusion
  192.9 0.4 fusion
  193.3 2.0 all-gather.4.cloned.1.call-done
  195.3 3.3 %fusion.19 = bf16[384,640]{1,0:T(8,128)(2,1)S(1)} fusion(bf16[2048,1920]{1,0:T(8,128)(2,1)} %all-gather.4.cloned.1.call-done, bf16[384,2048]{1,0:T(8,128)(2,1)S(1)} %bitcast_dynamic-update-slice_fusion, f32[2048]{0:T(1024)S(1)} %copy-done.13, f32[384]{0:T(512)S(1)} %add_rsqrt_fusion), kind=kOutput, calls=%fused_computation.27 | convolution fusion | flops 1010024448 | bytes 4695552 | tf_op jit(solution)/shard_map/dot_general | solution.py:76
  198.7 0.1 convert.48
  198.7 0.6 copy-done.12
  199.4 1.5 fusion.22
  200.8 0.1 convert.49
  200.9 0.3 fusion.42
  201.2 0.3 fusion.46
  201.5 0.3 fusion.49
  201.8 1.4 fusion.5
  203.2 0.1 fusion.65
  203.4 0.1 pad_maximum_fusion.1
  203.5 2.0 collective-permute-start.4
  205.4 0.2 select_bitcast_fusion.3
  205.7 2.0 collective-permute-done.4
  207.7 0.2 fusion.15
  207.9 16.4 %all_to_all.16 = bf16[4,384,256]{2,1,0:T(8,128)(2,1)S(1)} all-to-all(bf16[4,384,256]{2,1,0:T(8,128)(2,1)S(1)} %fusion.15), channel_id=1, replica_groups=mesh['gp'=1,'pair'=2,'fa'=8,'fb'=4,'tx'=4,'tc'=2] {'tx'}, dimensions={0} | all-to-all | bytes 1572864 | tf_op jit(solution)/shard_map/all_to_all | solution.py:52
  224.3 0.1 convert_reduce_fusion
  224.4 0.7 add_convert_fusion
  (32 shorter events, 0.2 us)
Async XLA Ops:
  6.5 188.8 %all-gather.4.cloned.1.call-start = ((), (), s32[]{:S(2)}) async-start(), calls=%async_computation.3 | async-start | bytes 8110080 | tf_op jit(solution)/shard_map/all_gather | solution.py:131
  10.8 4.8 %copy-start.5 = (bf16[64,128]{1,0:T(8,128)(2,1)S(1)}, bf16[64,128]{1,0:T(8,128)(2,1)}, u32[]{:S(2)}) copy-start(bf16[64,128]{1,0:T(8,128)(2,1)} %param.16) | copy-start | bytes 49156
  10.8 4.8 %copy-start.6 = (bf16[128,64]{0,1:T(8,128)(2,1)S(1)}, bf16[128,64]{0,1:T(8,128)(2,1)}, u32[]{:S(2)}) copy-start(bf16[128,64]{0,1:T(8,128)(2,1)} %param.19) | copy-start | bytes 49156
  10.8 4.8 %copy-start.7 = (bf16[64,128]{1,0:T(8,128)(2,1)S(1)}, bf16[64,128]{1,0:T(8,128)(2,1)}, u32[]{:S(2)}) copy-start(bf16[64,128]{1,0:T(8,128)(2,1)} %param.15) | copy-start | bytes 49156
  10.8 4.8 %copy-start.8 = (bf16[64,128]{1,0:T(8,128)(2,1)S(1)}, bf16[64,128]{1,0:T(8,128)(2,1)}, u32[]{:S(2)}) copy-start(bf16[64,128]{1,0:T(8,128)(2,1)} %param.17) | copy-start | bytes 49156
  10.8 129.4 %all-to-all-start = ((bf16[8,384,256]{1,2,0:T(8,128)(2,1)}), bf16[8,384,256]{1,2,0:T(8,128)(2,1)S(1)}, u32[]{:S(2)}, u32[]{:S(2)}) async-start(bf16[8,384,256]{1,2,0:T(8,128)(2,1)} %broadcast_in_dim.2), calls=%async_computation | async-start | bytes 3145728 | tf_op jit(solution)/shard_map/all_to_all | solution.py:22
  15.5 124.6 %copy-start.4 = (f32[2048]{0:T(1024)S(1)}, f32[2048]{0:T(1024)}, u32[]{:S(2)}) copy-start(f32[2048]{0:T(1024)} %param.14) | copy-start | bytes 24580
  15.5 124.6 %copy-start.11 = (f32[3,128]{1,0:T(4,128)S(1)}, f32[3,128]{1,0:T(4,128)}, u32[]{:S(2)}) copy-start(f32[3,128]{1,0:T(4,128)} %param.18) | copy-start | bytes 4612
  113.7 28.4 %collective-permute-start.1 = (bf16[2048,128]{1,0:T(8,128)(2,1)S(1)}, bf16[2048,128]{1,0:T(8,128)(2,1)}, u32[]{:S(2)}, u32[]{:S(2)}) collective-permute-start(bf16[2048,128]{1,0:T(8,128)(2,1)S(1)} %bitcast.135), channel_id=1, source_target_pairs={{0,256},{256,0},{1,257},{257,1},{2,258},{258,2},{3,259},{259,3},{4... | collective-permute-start | bytes 1572872 | tf_op jit(solution)/shard_map/ppermute | solution.py:28
  136.6 4.4 %copy-start.1 = (bf16[8,256,128]{2,1,0:T(8,128)(2,1)}, bf16[8,256,128]{2,1,0:T(8,128)(2,1)S(1)}, u32[]{:S(2)}) copy-start(bf16[8,256,128]{2,1,0:T(8,128)(2,1)S(1)} %all_gather.23) | copy-start | bytes 1572868
  136.6 11.1 %collective-permute-start = (bf16[2048,128]{1,0:T(8,128)(2,1)S(1)}, bf16[2048,128]{1,0:T(8,128)(2,1)S(1)}, u32[]{:S(2)}, u32[]{:S(2)}) collective-permute-start(bf16[2048,128]{1,0:T(8,128)(2,1)S(1)} %bitcast.130), channel_id=1, source_target_pairs={{0,256},{256,0},{1,257},{257,1},{2,258},{258,2},{3,259},{259,3},{4... | collective-permute-start | bytes 1572872 | tf_op jit(solution)/shard_map/ppermute | solution.py:28
  141.0 1.2 copy-start
  147.7 0.8 copy-start.2
  152.3 4.2 %collective-permute-start.2 = (bf16[4,384,256]{2,1,0:T(8,128)(2,1)S(1)}, bf16[4,384,256]{2,1,0:T(8,128)(2,1)S(1)}, u32[]{:S(2)}, u32[]{:S(2)}) collective-permute-start(bf16[4,384,256]{2,1,0:T(8,128)(2,1)S(1)} %pad_maximum_fusion), channel_id=1, source_target_pairs={{0,1},{1,0},{2,3},{3,2},{4,5},{5,4},{6,7},{7,6},{8,9},{9,8},{10,11... | collective-permute-start | bytes 2359304 | tf_op jit(solution)/shard_map/ppermute | solution.py:28
  156.7 17.1 %copy-start.3 = (bf16[384,256]{1,0:T(8,128)(2,1)S(1)}, bf16[384,256]{1,0:T(8,128)(2,1)}, u32[]{:S(2)}) copy-start(bf16[384,256]{1,0:T(8,128)(2,1)} %param.13) | copy-start | bytes 589828
  173.7 16.7 %copy-start.10 = (f32[2,640]{1,0:T(2,128)S(1)}, f32[2,640]{1,0:T(2,128)}, u32[]{:S(2)}) copy-start(f32[2,640]{1,0:T(2,128)} %param.24) | copy-start | bytes 15364
  173.7 16.7 %copy-start.9 = (f32[2,3,640]{2,0,1:T(2,128)S(1)}, f32[2,3,640]{2,0,1:T(2,128)}, u32[]{:S(2)}) copy-start(f32[2,3,640]{2,0,1:T(2,128)} %param.23) | copy-start | bytes 46084
  188.2 4.2 %collective-permute-start.3 = (bf16[4,384,256]{2,1,0:T(8,128)(2,1)S(1)}, bf16[4,384,256]{2,1,0:T(8,128)(2,1)S(1)}, u32[]{:S(2)}, u32[]{:S(2)}) collective-permute-start(bf16[4,384,256]{2,1,0:T(8,128)(2,1)S(1)} %bitcast.129), channel_id=1, source_target_pairs={{0,1},{1,0},{2,3},{3,2},{4,5},{5,4},{6,7},{7,6},{8,9},{9,8},{10,11... | collective-permute-start | bytes 2359304 | tf_op jit(solution)/shard_map/ppermute | solution.py:28
  192.7 2.6 %copy-start.13 = (f32[2048]{0:T(1024)S(1)}, f32[2048]{0:T(1024)}, u32[]{:S(2)}) copy-start(f32[2048]{0:T(1024)} %param.20) | copy-start | bytes 24580
  195.3 4.0 %copy-start.12 = (bf16[2048,1920]{1,0:T(8,128)(2,1)S(1)}, bf16[2048,1920]{1,0:T(8,128)(2,1)}, u32[]{:S(2)}) copy-start(bf16[2048,1920]{1,0:T(8,128)(2,1)} %all-gather.4.cloned.1.call-done) | copy-start | bytes 23592964
  203.5 4.2 %collective-permute-start.4 = (bf16[4,384,256]{2,1,0:T(8,128)(2,1)S(1)}, bf16[4,384,256]{2,1,0:T(8,128)(2,1)S(1)}, u32[]{:S(2)}, u32[]{:S(2)}) collective-permute-start(bf16[4,384,256]{2,1,0:T(8,128)(2,1)S(1)} %pad_maximum_fusion.1), channel_id=1, source_target_pairs={{0,1},{1,0},{2,3},{3,2},{4,5},{5,4},{6,7},{7,6},{8,9},{9,8},{10,11... | collective-permute-start | bytes 2359304 | tf_op jit(solution)/shard_map/ppermute | solution.py:28
Sparse Core Ops, SparseCore 0:
  9.4 185.8 all-gather.3

commit v3 on v2

--- a/solution.py
+++ b/solution.py
@@ -1,6 +1,8 @@
 import jax
 import jax.numpy as jnp
 from jax import lax
+from jax.experimental import pallas as pl
+from jax.experimental.pallas import tpu as pltpu
 from jax.sharding import Mesh
 from jax.sharding import PartitionSpec as P
 
@@ -38,6 +40,13 @@
     other = swapped(own, "tc")
     pieces = [piece for chip in range(own.shape[0]) for piece in by_core(own[chip], other[chip])]
     return jnp.concatenate(pieces, axis=1)
+
+
+def pairs_and_summed(keep, send):
+    received = swapped(send, "tc")
+    pairs = (keep.astype(jnp.float32) + received.astype(jnp.float32)).astype(jnp.bfloat16)
+    parts = lax.all_to_all(pairs, "tx", 0, 0, tiled=True)
+    return jnp.sum(parts.astype(jnp.float32), axis=0)
 
 
 def sent_and_summed(terms):
@@ -47,10 +56,7 @@
     chosen = [by_core(*blocks[k : k + CORES]) for k in range(0, chips * CORES, CORES)]
     keep = jnp.stack([pair[0] for pair in chosen])
     send = jnp.stack([pair[1] for pair in chosen])
-    received = swapped(send.astype(jnp.bfloat16), "tc")
-    pairs = (keep + received.astype(jnp.float32)).astype(jnp.bfloat16)
-    parts = lax.all_to_all(pairs, "tx", 0, 0, tiled=True)
-    return jnp.sum(parts.astype(jnp.float32), axis=0)
+    return pairs_and_summed(keep, send.astype(jnp.bfloat16))
 
 
 def conv_positions(values, taps):
@@ -80,6 +86,110 @@
     return lax.dot_general(
         left, right_t, (((1,), (1,)), ((), ())), preferred_element_type=jnp.float32
     )
+
+
+LANES = 128
+
+
+def ffn_body(core, normed, taps, bias, weights, keep, send, up, down, hidden, sems):
+    rows, features = normed.shape
+    wide = hidden.shape[1]
+    blocks = wide // LANES
+    chips, _, share = keep.shape
+
+    def up_copy(block, half):
+        start = half * wide + block * LANES
+        return pltpu.make_async_copy(
+            weights.at[:, start : start + LANES],
+            up.at[block, :, half * LANES : (half + 1) * LANES],
+            sems.at[2 * block + half],
+        )
+
+    def down_copy(part):
+        piece = pl.ds(part * share, share)
+        return pltpu.make_async_copy(
+            weights.at[piece, 2 * wide : 3 * wide], down.at[piece], sems.at[2 * blocks + part]
+        )
+
+    for block in range(blocks):
+        up_copy(block, 0).start()
+        up_copy(block, 1).start()
+    for part in range(CORES * chips):
+        down_copy(part).start()
+
+    length = rows // SEQS_DEV
+    place = lax.broadcasted_iota(jnp.int32, (rows, LANES), 0) % length
+
+    def conv(values, half, block):
+        cols = slice(block * LANES, (block + 1) * LANES)
+        values = values.astype(jnp.bfloat16).astype(jnp.float32)
+        one = jnp.where(place >= 1, pltpu.roll(values, 1, 0), 0.0)
+        two = jnp.where(place >= 2, pltpu.roll(values, 2, 0), 0.0)
+        summed = (
+            two * taps[half, 0:1, cols] + one * taps[half, 1:2, cols] + values * taps[half, 2:3, cols]
+        )
+        return summed + bias[half : half + 1, cols]
+
+    for block in range(blocks):
+        up_copy(block, 0).wait()
+        up_copy(block, 1).wait()
+        both = jnp.dot(normed[...], up[block], preferred_element_type=jnp.float32)
+        gate = conv(both[:, :LANES], 0, block)
+        value = conv(both[:, LANES:], 1, block)
+        act = gate / (1.0 + jnp.exp(-gate))
+        hidden[:, block * LANES : (block + 1) * LANES] = (act * value).astype(jnp.bfloat16)
+
+    for part in range(CORES * chips):
+        down_copy(part).wait()
+
+    def terms(chip, side):
+        piece = pl.ds(pl.multiple_of((CORES * chip + side) * share, share), share)
+        return lax.dot_general(
+            hidden[...], down[piece], (((1,), (1,)), ((), ())), preferred_element_type=jnp.float32
+        )
+
+    own = core[0]
+    for chip in range(chips):
+        send[chip] = terms(chip, 1 - own).astype(send.dtype)
+    for chip in range(chips):
+        keep[chip] = terms(chip, own).astype(keep.dtype)
+
+
+def ffn_terms(normed, taps, bias, weights):
+    rows, features = normed.shape
+    wide = bias.shape[1]
+    chips = lax.axis_size("tx")
+    share = features // (chips * CORES)
+    blocks = wide // LANES
+    vmem = pl.BlockSpec(memory_space=pltpu.VMEM)
+    return pl.pallas_call(
+        ffn_body,
+        in_specs=[
+            pl.BlockSpec(memory_space=pltpu.SMEM),
+            vmem,
+            vmem,
+            vmem,
+            pl.BlockSpec(memory_space=pltpu.HBM),
+        ],
+        out_specs=[vmem, vmem],
+        out_shape=[
+            jax.ShapeDtypeStruct((chips, rows, share), jnp.float32),
+            jax.ShapeDtypeStruct((chips, rows, share), jnp.bfloat16),
+        ],
+        scratch_shapes=[
+            pltpu.VMEM((blocks, features, 2 * LANES), jnp.bfloat16),
+            pltpu.VMEM((features, wide), jnp.bfloat16),
+            pltpu.VMEM((rows, wide), jnp.bfloat16),
+            pltpu.SemaphoreType.DMA((2 * blocks + CORES * chips,)),
+        ],
+        compiler_params=pltpu.CompilerParams(vmem_limit_bytes=24 * 1024 * 1024),
+        cost_estimate=pl.CostEstimate(
+            flops=2 * rows * features * 3 * wide,
+            bytes_accessed=2 * features * 3 * wide + 2 * rows * features,
+            transcendentals=rows * wide,
+        ),
+        name="ffn_terms",
+    )(lax.axis_index("tc").astype(jnp.int32).reshape(1), normed, taps, bias, pltpu.with_memory_space_constraint(weights, pltpu.HBM))
 
 
 def near_gather(far):
@@ -127,7 +237,6 @@
     w_down,
     paired,
 ):
-    hidden_width = w_gate.shape[1]
     ffn_full = lax.all_gather(side_by_side((w_gate, w_value, w_down.T)), FS, axis=0, tiled=True)
     whole = gathered_copies(tokens, TP)
     early_a, early_b, outer_full, mix_full = mixer_weights(
@@ -141,12 +250,7 @@
     resid = (tokens.astype(jnp.float32) + mix_sum).astype(jnp.bfloat16)
     whole_ffn = gathered_features(resid)
     normed_ffn = rms_norm(whole_ffn, ffn_gain)
-    gate = rounded(dot(normed_ffn, ffn_full[:, :hidden_width]))
-    value = rounded(dot(normed_ffn, ffn_full[:, hidden_width : 2 * hidden_width]))
-    gate_conv = conv_positions(gate, up_taps[0]) + up_bias[0]
-    value_conv = conv_positions(value, up_taps[1]) + up_bias[1]
-    hidden = (jax.nn.silu(gate_conv) * value_conv).astype(jnp.bfloat16)
-    ffn_sum = sent_and_summed(dot_t(hidden, ffn_full[:, 2 * hidden_width :]))
+    ffn_sum = pairs_and_summed(*ffn_terms(normed_ffn, up_taps, up_bias, ffn_full))
     return (resid.astype(jnp.float32) + ffn_sum).astype(jnp.bfloat16)
 
 

time: 233 us -> 233 us (level)
  Pallas kernels: 0 us -> 8.59 us
  matrix products: 12.4 us -> 6.17 us
    pallas_call x0 -> x1, Pallas kernels: none -> 8.59 us  [ffn_terms(): pl.pallas_call(ffn_body, in_specs=[pl.BlockSpec(memory_space=pltpu.SMEM),...]
    dot_general x4 -> x2, matrix products: 7.48 us -> 2.67 us  [dot(): return jnp.dot(left, right, preferred_element_type=jnp.float32)]
    dot_general x2 -> x1, matrix products: 4.92 us -> 3.51 us  [dot_t(): lax.dot_general(left, right_t, (((1,), (1,)), ((), ())), preferred_elemen...]
where the time goes in v3:
time: 233 us
  blocking collectives  167 us (72%)
  starting transfers between devices  16.7 us (7%)
  between operations  13.8 us (6%)
  waiting for transfers between devices  10.8 us (5%)
  Pallas kernels  8.59 us (4%)
  matrix products  6.17 us (3%)
  other arithmetic  5.75 us (2%)
  local copies, waits for them, and re-layouts  3.72 us (2%)
    all_gather x1, blocking collectives, mixer_weights(): far = lax.all_gather(side_by_side((early, late)), 'fa', axis=0)  74.3 us
    all_gather x2, blocking collectives, near_gather(): wide = lax.all_gather(far, 'fb', axis=1, tiled=True)  44.5 us
    all_to_all x2, blocking collectives, pairs_and_summed(): parts = lax.all_to_all(pairs, 'tx', 0, 0, tiled=True)  33.8 us
    all_gather x1, blocking collectives, gathered_features(): own = lax.all_gather(value, 'tx', axis=0)  14.4 us
    ppermute x5, starting transfers between devices, swapped(): return lax.ppermute(value, axis, [(0, 1), (1, 0)])  12 us
    ppermute x5, waiting for transfers between devices, swapped(): return lax.ppermute(value, axis, [(0, 1), (1, 0)])  9.6 us
    pallas_call x1, Pallas kernels, ffn_terms(): pl.pallas_call(ffn_body, in_specs=[pl.BlockSpec(memory_space=pltpu.SMEM),...  8.59 us
    all_to_all x1, starting transfers between devices, gathered_copies(): lax.all_to_all(copies, axis, split_axis=0, concat_axis=0, tiled=True)  4.73 us
  transfers between devices with their start and end apart: 7, of which 5 were waited for; matrix products, arithmetic and copies ran while one was open for 5% of the time, Pallas kernels for 0%

profile of v3, /device:TPU:40, one launch (start us, length us, event | category | flops | bytes accessed | tf_op | source)
XLA Modules:
  0.0 232.6 jit_solution(2355746823320694135)
XLA Ops:
  6.5 0.0 all-gather.4.cloned.1.call-start
  6.6 1.7 pad_maximum_fusion.1
  8.3 0.1 all-gather.4.cloned.1.call-update
  8.3 1.1 copy.15
  9.4 1.4 broadcast_in_dim.2
  10.8 4.7 %all-to-all-start = ((bf16[8,384,256]{1,2,0:T(8,128)(2,1)}), bf16[8,384,256]{1,2,0:T(8,128)(2,1)S(1)}, u32[]{:S(2)}, u32[]{:S(2)}) async-start(bf16[8,384,256]{1,2,0:T(8,128)(2,1)} %broadcast_in_dim.2), calls=%async_computation | async-start | bytes 3145728 | tf_op jit(solution)/shard_map/all_to_all | solution.py:24
  15.5 0.0 copy-start.12
  15.5 0.0 copy-done.6
  15.6 0.0 copy-done.7
  15.6 0.0 copy-done.8
  15.6 0.0 copy-done.9
  15.6 74.3 %all-gather = bf16[512,256]{1,0:T(8,128)(2,1)S(1)} all-gather(bf16[64,256]{1,0:T(8,128)(2,1)S(1)} %pad_maximum_fusion.2), channel_id=2, replica_groups=mesh['gp'=1,'pair'=2,'fa'=8,'fb'=4,'tx'=4,'tc'=2] {'fa'}, dimensions={0}, use_global_device_ids=true | all-gather | bytes 294912 | tf_op jit(solution)/shard_map/all_gather | solution.py:214
  89.9 0.1 fusion.40
  90.0 23.9 %all_gather.24 = bf16[8,256,128]{2,1,0:T(8,128)(2,1)S(1)} all-gather(bf16[8,64,128]{2,1,0:T(8,128)(2,1)S(1)} %get-tuple-element.18), channel_id=1, replica_groups=mesh['gp'=1,'pair'=2,'fa'=8,'fb'=4,'tx'=4,'tc'=2] {'fb'}, dimensions={1}, use_global_device_ids=true | all-gather | bytes 655360 | tf_op jit(solution)/shard_map/all_gather | solution.py:196
  113.9 1.9 collective-permute-start.1
  115.8 20.7 %all_gather.23 = bf16[8,256,128]{2,1,0:T(8,128)(2,1)S(1)} all-gather(bf16[8,64,128]{2,1,0:T(8,128)(2,1)S(1)} %get-tuple-element.17), channel_id=1, replica_groups=mesh['gp'=1,'pair'=2,'fa'=8,'fb'=4,'tx'=4,'tc'=2] {'fb'}, dimensions={1}, use_global_device_ids=true | all-gather | bytes 655360 | tf_op jit(solution)/shard_map/all_gather | solution.py:196
  136.5 4.0 %collective-permute-start = (bf16[2048,128]{1,0:T(8,128)(2,1)S(1)}, bf16[2048,128]{1,0:T(8,128)(2,1)S(1)}, u32[]{:S(2)}, u32[]{:S(2)}) collective-permute-start(bf16[2048,128]{1,0:T(8,128)(2,1)S(1)} %bitcast.100), channel_id=1, source_target_pairs={{0,256},{256,0},{1,257},{257,1},{2,258},{258,2},{3,259},{259,3},{4... | collective-permute-start | bytes 1572872 | tf_op jit(solution)/shard_map/ppermute | solution.py:30
  140.5 0.0 copy-done.5
  140.6 0.0 copy-done.12
  140.6 0.0 all-to-all-done
  140.6 0.4 multiply_reduce_fusion
  141.0 0.4 fusion.4
  141.4 0.0 copy-done.2
  141.4 0.0 copy-start.1
  141.5 1.0 fusion.18
  142.5 0.0 collective-permute-done.1
  142.5 0.2 copy-done.1
  142.7 1.7 fusion.22
  144.3 0.1 fusion.34
  144.4 3.3 %collective-permute-done = bf16[2048,128]{1,0:T(8,128)(2,1)S(1)} collective-permute-done((bf16[2048,128]{1,0:T(8,128)(2,1)S(1)}, bf16[2048,128]{1,0:T(8,128)(2,1)S(1)}, u32[]{:S(2)}, u32[]{:S(2)}) %collective-permute-start) | collective-permute-done | bytes 524320 | tf_op jit(solution)/shard_map/ppermute | solution.py:30
  147.7 0.8 copy-done.3
  148.5 3.5 %fusion.26 = f32[384,2048]{1,0:T(8,128)S(1)} fusion(f32[384,128]{1,0:T(8,128)S(1)} %bitcast.104, bf16[384,2048]{0,1:T(8,128)(2,1)} %copy-done.1, bf16[2048,128]{1,0:T(8,128)(2,1)} %copy-done.3, bf16[2048,128]{1,0:T(8,128)(2,1)} %bitcast.101, pred[]{:T(512)S(6)} %eq.5), kind=kOutput, calls=%fused_computation.30 | convolution fusion | flops 403374080 | bytes 5963777 | tf_op jit(solution)/shard_map/dot_general | solution.py:86
  152.0 0.1 fusion.36
  152.2 0.1 pad_maximum_fusion
  152.3 2.0 collective-permute-start.2
  154.2 0.2 select_bitcast_fusion.3
  154.4 2.0 collective-permute-done.2
  156.5 0.2 fusion.8
  156.7 0.0 copy-start.4
  156.7 17.1 %all_to_all.15 = bf16[4,384,256]{2,1,0:T(8,128)(2,1)S(1)} all-to-all(bf16[4,384,256]{2,1,0:T(8,128)(2,1)S(1)} %fusion.8), channel_id=1, replica_groups=mesh['gp'=1,'pair'=2,'fa'=8,'fb'=4,'tx'=4,'tc'=2] {'tx'}, dimensions={0} | all-to-all | bytes 1572864 | tf_op jit(solution)/shard_map/all_to_all | solution.py:48
  173.8 0.1 convert_reduce_fusion.1
  174.0 14.4 %all-gather.1 = bf16[1536,256]{1,0:T(8,128)(2,1)S(1)} all-gather(bf16[384,256]{1,0:T(8,128)(2,1)S(1)} %add_convert_fusion.2), channel_id=3, replica_groups=mesh['gp'=1,'pair'=2,'fa'=8,'fb'=4,'tx'=4,'tc'=2] {'tx'}, dimensions={0}, use_global_device_ids=true | all-gather | bytes 983040 | tf_op jit(solution)/shard_map/all_gather | solution.py:39
  188.4 2.1 collective-permute-start.3
  190.6 2.0 collective-permute-done.3
  192.6 0.1 bitcast_dynamic-update-slice_fusion.7
  192.7 0.1 bitcast_dynamic-update-slice_fusion.6
  192.7 0.1 bitcast_dynamic-update-slice_fusion.5
  192.8 0.1 bitcast_dynamic-update-slice_fusion.4
  192.8 0.1 bitcast_dynamic-update-slice_fusion.3
  192.9 0.0 copy-start.11
  192.9 0.1 bitcast_dynamic-update-slice_fusion.2
  193.0 0.1 bitcast_dynamic-update-slice_fusion.1
  193.0 0.1 bitcast_dynamic-update-slice_fusion
  193.1 0.4 fusion
  193.5 0.1 copy-done.11
  193.6 0.4 fusion.2.normed
  194.0 1.2 all-gather.4.cloned.1.call-done.weights
  195.2 8.6 %ffn_terms.1 = (f32[4,384,256]{2,1,0:T(8,128)S(1)}, bf16[4,384,256]{2,1,0:T(8,128)(2,1)S(1)}) custom-call(s32[1]{0:T(128)} %bitcast.21.core, bf16[384,2048]{1,0:T(8,128)(2,1)S(1)} %fusion.2.normed, f32[2,3,640]{2,1,0:T(4,128)S(1)} %copy.17.taps, f32[2,640]{1,0:T(2,128)S(1)} %copy-done, bf16[2048,1920]{1,0:T(8,128)(2,1)} %all-gather.4.cloned.1.call-done.weights), custom_call_target="tpu_custom_call" | custom-call | flops 3019898880 | bytes 9437184 | tf_op jit(solution)/shard_map/ffn_terms/pallas_call | solution.py:165
  203.8 2.0 collective-permute-start.4
  205.8 2.3 collective-permute-done.4
  208.0 0.2 add_convert_fusion
  208.3 16.6 %all_to_all.16 = bf16[4,384,256]{2,1,0:T(8,128)(2,1)S(1)} all-to-all(bf16[4,384,256]{2,1,0:T(8,128)(2,1)S(1)} %add_convert_fusion), channel_id=1, replica_groups=mesh['gp'=1,'pair'=2,'fa'=8,'fb'=4,'tx'=4,'tc'=2] {'tx'}, dimensions={0} | all-to-all | bytes 1572864 | tf_op jit(solution)/shard_map/all_to_all | solution.py:48
  224.9 0.1 convert_reduce_fusion
  225.0 0.7 add_convert_fusion.1
  (20 shorter events, 0.1 us)
Async XLA Ops:
  6.5 188.7 %all-gather.4.cloned.1.call-start = ((), (), s32[]{:S(2)}) async-start(), calls=%async_computation.3 | async-start | bytes 8110080 | tf_op jit(solution)/shard_map/all_gather | solution.py:240
  10.8 4.8 %copy-start.6 = (bf16[64,128]{1,0:T(8,128)(2,1)S(1)}, bf16[64,128]{1,0:T(8,128)(2,1)}, u32[]{:S(2)}) copy-start(bf16[64,128]{1,0:T(8,128)(2,1)} %param.16) | copy-start | bytes 49156
  10.8 4.8 %copy-start.7 = (bf16[128,64]{0,1:T(8,128)(2,1)S(1)}, bf16[128,64]{0,1:T(8,128)(2,1)}, u32[]{:S(2)}) copy-start(bf16[128,64]{0,1:T(8,128)(2,1)} %param.19) | copy-start | bytes 49156
  10.8 4.8 %copy-start.8 = (bf16[64,128]{1,0:T(8,128)(2,1)S(1)}, bf16[64,128]{1,0:T(8,128)(2,1)}, u32[]{:S(2)}) copy-start(bf16[64,128]{1,0:T(8,128)(2,1)} %param.15) | copy-start | bytes 49156
  10.8 4.8 %copy-start.9 = (bf16[64,128]{1,0:T(8,128)(2,1)S(1)}, bf16[64,128]{1,0:T(8,128)(2,1)}, u32[]{:S(2)}) copy-start(bf16[64,128]{1,0:T(8,128)(2,1)} %param.17) | copy-start | bytes 49156
  10.8 129.8 %all-to-all-start = ((bf16[8,384,256]{1,2,0:T(8,128)(2,1)}), bf16[8,384,256]{1,2,0:T(8,128)(2,1)S(1)}, u32[]{:S(2)}, u32[]{:S(2)}) async-start(bf16[8,384,256]{1,2,0:T(8,128)(2,1)} %broadcast_in_dim.2), calls=%async_computation | async-start | bytes 3145728 | tf_op jit(solution)/shard_map/all_to_all | solution.py:24
  15.5 125.0 %copy-start.5 = (f32[2048]{0:T(1024)S(1)}, f32[2048]{0:T(1024)}, u32[]{:S(2)}) copy-start(f32[2048]{0:T(1024)} %param.14) | copy-start | bytes 24580
  15.5 125.0 %copy-start.12 = (f32[3,128]{1,0:T(4,128)S(1)}, f32[3,128]{1,0:T(4,128)}, u32[]{:S(2)}) copy-start(f32[3,128]{1,0:T(4,128)} %param.18) | copy-start | bytes 4612
  113.9 28.6 %collective-permute-start.1 = (bf16[2048,128]{1,0:T(8,128)(2,1)S(1)}, bf16[2048,128]{1,0:T(8,128)(2,1)}, u32[]{:S(2)}, u32[]{:S(2)}) collective-permute-start(bf16[2048,128]{1,0:T(8,128)(2,1)S(1)} %bitcast.105), channel_id=1, source_target_pairs={{0,256},{256,0},{1,257},{257,1},{2,258},{258,2},{3,259},{259,3},{4... | collective-permute-start | bytes 1572872 | tf_op jit(solution)/shard_map/ppermute | solution.py:30
  136.5 4.9 %copy-start.2 = (bf16[8,256,128]{2,1,0:T(8,128)(2,1)}, bf16[8,256,128]{2,1,0:T(8,128)(2,1)S(1)}, u32[]{:S(2)}) copy-start(bf16[8,256,128]{2,1,0:T(8,128)(2,1)S(1)} %all_gather.23) | copy-start | bytes 1572868
  136.5 11.2 %collective-permute-start = (bf16[2048,128]{1,0:T(8,128)(2,1)S(1)}, bf16[2048,128]{1,0:T(8,128)(2,1)S(1)}, u32[]{:S(2)}, u32[]{:S(2)}) collective-permute-start(bf16[2048,128]{1,0:T(8,128)(2,1)S(1)} %bitcast.100), channel_id=1, source_target_pairs={{0,256},{256,0},{1,257},{257,1},{2,258},{258,2},{3,259},{259,3},{4... | collective-permute-start | bytes 1572872 | tf_op jit(solution)/shard_map/ppermute | solution.py:30
  141.4 1.2 copy-start.1
  147.7 0.8 copy-start.3
  152.3 4.2 %collective-permute-start.2 = (bf16[4,384,256]{2,1,0:T(8,128)(2,1)S(1)}, bf16[4,384,256]{2,1,0:T(8,128)(2,1)S(1)}, u32[]{:S(2)}, u32[]{:S(2)}) collective-permute-start(bf16[4,384,256]{2,1,0:T(8,128)(2,1)S(1)} %pad_maximum_fusion), channel_id=1, source_target_pairs={{0,1},{1,0},{2,3},{3,2},{4,5},{5,4},{6,7},{7,6},{8,9},{9,8},{10,11... | collective-permute-start | bytes 2359304 | tf_op jit(solution)/shard_map/ppermute | solution.py:30
  156.7 17.3 %copy-start.4 = (bf16[384,256]{1,0:T(8,128)(2,1)S(1)}, bf16[384,256]{1,0:T(8,128)(2,1)}, u32[]{:S(2)}) copy-start(bf16[384,256]{1,0:T(8,128)(2,1)} %param.13) | copy-start | bytes 589828
  173.8 16.7 %copy-start.10 = (f32[2,3,640]{2,0,1:T(2,128)S(1)}, f32[2,3,640]{2,0,1:T(2,128)}, u32[]{:S(2)}) copy-start(f32[2,3,640]{2,0,1:T(2,128)} %param.23) | copy-start | bytes 46084
  188.4 4.2 %collective-permute-start.3 = (bf16[4,384,256]{2,1,0:T(8,128)(2,1)S(1)}, bf16[4,384,256]{2,1,0:T(8,128)(2,1)S(1)}, u32[]{:S(2)}, u32[]{:S(2)}) collective-permute-start(bf16[4,384,256]{2,1,0:T(8,128)(2,1)S(1)} %bitcast.99), channel_id=1, source_target_pairs={{0,1},{1,0},{2,3},{3,2},{4,5},{5,4},{6,7},{7,6},{8,9},{9,8},{10,11... | collective-permute-start | bytes 2359304 | tf_op jit(solution)/shard_map/ppermute | solution.py:30
  192.9 0.7 copy-start.11
  193.6 1.6 copy-start
  203.8 4.2 %collective-permute-start.4 = (bf16[4,384,256]{2,1,0:T(8,128)(2,1)S(1)}, bf16[4,384,256]{2,1,0:T(8,128)(2,1)S(1)}, u32[]{:S(2)}, u32[]{:S(2)}) collective-permute-start(bf16[4,384,256]{2,1,0:T(8,128)(2,1)S(1)} %get-tuple-element.8), channel_id=1, source_target_pairs={{0,1},{1,0},{2,3},{3,2},{4,5},{5,4},{6,7},{7,6},{8,9},{9,8},{10,11... | collective-permute-start | bytes 2359304 | tf_op jit(solution)/shard_map/ppermute | solution.py:30
Sparse Core Ops, SparseCore 0:
  9.4 185.7 all-gather.3

commit v4 on v2

--- a/solution.py
+++ b/solution.py
@@ -1,6 +1,8 @@
 import jax
 import jax.numpy as jnp
 from jax import lax
+from jax.experimental import pallas as pl
+from jax.experimental.pallas import tpu as pltpu
 from jax.sharding import Mesh
 from jax.sharding import PartitionSpec as P
 
@@ -38,6 +40,13 @@
     other = swapped(own, "tc")
     pieces = [piece for chip in range(own.shape[0]) for piece in by_core(own[chip], other[chip])]
     return jnp.concatenate(pieces, axis=1)
+
+
+def pairs_and_summed(keep, send):
+    received = swapped(send, "tc")
+    pairs = (keep + received.astype(jnp.float32)).astype(jnp.bfloat16)
+    parts = lax.all_to_all(pairs, "tx", 0, 0, tiled=True)
+    return jnp.sum(parts.astype(jnp.float32), axis=0)
 
 
 def sent_and_summed(terms):
@@ -47,10 +56,7 @@
     chosen = [by_core(*blocks[k : k + CORES]) for k in range(0, chips * CORES, CORES)]
     keep = jnp.stack([pair[0] for pair in chosen])
     send = jnp.stack([pair[1] for pair in chosen])
-    received = swapped(send.astype(jnp.bfloat16), "tc")
-    pairs = (keep + received.astype(jnp.float32)).astype(jnp.bfloat16)
-    parts = lax.all_to_all(pairs, "tx", 0, 0, tiled=True)
-    return jnp.sum(parts.astype(jnp.float32), axis=0)
+    return pairs_and_summed(keep, send.astype(jnp.bfloat16))
 
 
 def conv_positions(values, taps):
@@ -106,9 +112,57 @@
     early_other = swapped(early_own, "pair")
     late_own = near_gather(far[:, :, width:])
     late_other = swapped(late_own, "pair")
-    outer_full = jnp.where(first, late_own, late_other)
-    mix_full = jnp.where(first, late_other, late_own)
-    return early_own, early_other, outer_full, mix_full
+    return early_own, early_other, late_own, late_other
+
+
+def mixer_body(where, normed, product, taps, late_a, late_b, keep, send):
+    rows = normed.shape[0]
+    chips, _, share = keep.shape
+    first = where[0] == 0
+    own = where[1]
+    outer_full = jnp.where(first, late_a[...], late_b[...])
+    outer = rounded(dot(normed[...], outer_full))
+    values = product[...]
+    place = lax.broadcasted_iota(jnp.int32, values.shape, 0) % (rows // SEQS_DEV)
+    one = jnp.where(place >= 1, pltpu.roll(values, 1, 0), 0.0)
+    two = jnp.where(place >= 2, pltpu.roll(values, 2, 0), 0.0)
+    conv = two * taps[0:1, :] + one * taps[1:2, :] + values * taps[2:3, :]
+    mixed = (outer * conv).astype(jnp.bfloat16)
+
+    def terms(chip, side):
+        piece = pl.ds(pl.multiple_of((CORES * chip + side) * share, share), share)
+        return dot_t(mixed, jnp.where(first, late_b[piece, :], late_a[piece, :]))
+
+    for chip in range(chips):
+        send[chip] = terms(chip, 1 - own).astype(send.dtype)
+    for chip in range(chips):
+        keep[chip] = terms(chip, own)
+
+
+def mixer_terms(normed, product, taps, late_a, late_b, paired):
+    rows, features = normed.shape
+    width = product.shape[1]
+    chips = lax.axis_size("tx")
+    share = features // (chips * CORES)
+    pair = lax.axis_index("pair") if paired else 0 * lax.axis_index("tc")
+    where = jnp.stack([pair, lax.axis_index("tc")]).astype(jnp.int32)
+    vmem = pl.BlockSpec(memory_space=pltpu.VMEM)
+    return pl.pallas_call(
+        mixer_body,
+        in_specs=[pl.BlockSpec(memory_space=pltpu.SMEM), vmem, vmem, vmem, vmem, vmem],
+        out_specs=[vmem, vmem],
+        out_shape=[
+            jax.ShapeDtypeStruct((chips, rows, share), jnp.float32),
+            jax.ShapeDtypeStruct((chips, rows, share), jnp.bfloat16),
+        ],
+        compiler_params=pltpu.CompilerParams(vmem_limit_bytes=16 * 1024 * 1024),
+        cost_estimate=pl.CostEstimate(
+            flops=4 * rows * features * width,
+            bytes_accessed=2 * features * (rows + 2 * width) + 6 * rows * features,
+            transcendentals=0,
+        ),
+        name="mixer_terms",
+    )(where, normed, product, taps, late_a, late_b)
 
 
 def on_device(
@@ -127,26 +181,26 @@
     w_down,
     paired,
 ):
-    hidden_width = w_gate.shape[1]
-    ffn_full = lax.all_gather(side_by_side((w_gate, w_value, w_down.T)), FS, axis=0, tiled=True)
+    shards = jnp.stack((w_gate, w_value, w_down.T))
+    gate_full, value_full, down_t = lax.all_gather(shards, FS, axis=1, tiled=True)
     whole = gathered_copies(tokens, TP)
-    early_a, early_b, outer_full, mix_full = mixer_weights(
+    early_a, early_b, late_a, late_b = mixer_weights(
         w_signal, w_outer_gate, w_inner_gate, w_mix_out.T, paired
     )
     normed = rms_norm(whole, mix_gain)
     product = rounded(dot(normed, early_a)) * rounded(dot(normed, early_b))
-    outer = rounded(dot(normed, outer_full))
-    mixed = (outer * conv_positions(product, mix_taps)).astype(jnp.bfloat16)
-    mix_sum = sent_and_summed(dot_t(mixed, mix_full))
+    mix_sum = pairs_and_summed(
+        *mixer_terms(normed, product, mix_taps, late_a, late_b, paired)
+    )
     resid = (tokens.astype(jnp.float32) + mix_sum).astype(jnp.bfloat16)
     whole_ffn = gathered_features(resid)
     normed_ffn = rms_norm(whole_ffn, ffn_gain)
-    gate = rounded(dot(normed_ffn, ffn_full[:, :hidden_width]))
-    value = rounded(dot(normed_ffn, ffn_full[:, hidden_width : 2 * hidden_width]))
+    gate = rounded(dot(normed_ffn, gate_full))
+    value = rounded(dot(normed_ffn, value_full))
     gate_conv = conv_positions(gate, up_taps[0]) + up_bias[0]
     value_conv = conv_positions(value, up_taps[1]) + up_bias[1]
     hidden = (jax.nn.silu(gate_conv) * value_conv).astype(jnp.bfloat16)
-    ffn_sum = sent_and_summed(dot_t(hidden, ffn_full[:, 2 * hidden_width :]))
+    ffn_sum = sent_and_summed(dot_t(hidden, down_t))
     return (resid.astype(jnp.float32) + ffn_sum).astype(jnp.bfloat16)
 
 

time: 233 us -> 232 us (level)
  matrix products: 12.4 us -> 8.45 us
  waiting for transfers between devices: 11.8 us -> 14.9 us
  Pallas kernels: 0 us -> 2.36 us
    dot_general x2 -> x1, matrix products: 4.92 us -> 1.41 us  [dot_t(): lax.dot_general(left, right_t, (((1,), (1,)), ((), ())), preferred_elemen...]
    all_gather x1, waiting for transfers between devices: 2.02 us -> 5.29 us  [on_device(): lax.all_gather(shards, FS, axis=1, tiled=True)]
    pallas_call x0 -> x1, Pallas kernels: none -> 2.36 us  [mixer_terms(): pl.pallas_call(mixer_body, in_specs=[pl.BlockSpec(memory_space=pltpu.SMEM...]
  transfers between devices with their start and end apart: 7 -> 7, of which waited for: 5 -> 5; matrix products, arithmetic and copies ran while one was open for 5% -> 3% of each run, Pallas kernels for 0% -> 1%
where the time goes in v4:
time: 232 us
  blocking collectives  165 us (71%)
  starting transfers between devices  16.7 us (7%)
  waiting for transfers between devices  14.9 us (6%)
  between operations  13.8 us (6%)
  matrix products  8.45 us (4%)
  other arithmetic  6.45 us (3%)
  local copies, waits for them, and re-layouts  3.41 us (1%)
  Pallas kernels  2.36 us (1%)
    all_gather x1, blocking collectives, mixer_weights(): far = lax.all_gather(side_by_side((early, late)), 'fa', axis=0)  74.2 us
    all_gather x2, blocking collectives, near_gather(): wide = lax.all_gather(far, 'fb', axis=1, tiled=True)  44.5 us
    all_to_all x2, blocking collectives, pairs_and_summed(): parts = lax.all_to_all(pairs, 'tx', 0, 0, tiled=True)  32.4 us
    all_gather x1, blocking collectives, gathered_features(): own = lax.all_gather(value, 'tx', axis=0)  14.4 us
    ppermute x5, starting transfers between devices, swapped(): return lax.ppermute(value, axis, [(0, 1), (1, 0)])  12 us
    ppermute x5, waiting for transfers between devices, swapped(): return lax.ppermute(value, axis, [(0, 1), (1, 0)])  9.61 us
    dot_general x4, matrix products, dot(): return jnp.dot(left, right, preferred_element_type=jnp.float32)  7.04 us
    all_gather x1, waiting for transfers between devices, on_device(): lax.all_gather(shards, FS, axis=1, tiled=True)  5.29 us
  transfers between devices with their start and end apart: 7, of which 5 were waited for; matrix products, arithmetic and copies ran while one was open for 3% of the time, Pallas kernels for 1%

profile of v4, /device:TPU:40, one launch (start us, length us, event | category | flops | bytes accessed | tf_op | source)
XLA Modules:
  0.0 231.6 jit_solution(7695821189863637372)
XLA Ops:
  6.5 0.0 all-gather.4.cloned.1.call-start
  6.6 1.7 pad_maximum_fusion.1
  8.2 0.1 all-gather.4.cloned.1.call-update
  8.3 2.3 broadcast_in_dim.2
  10.6 4.7 %all-to-all-start = ((bf16[8,384,256]{2,1,0:T(8,128)(2,1)}), bf16[8,384,256]{2,1,0:T(8,128)(2,1)S(1)}, u32[]{:S(2)}, u32[]{:S(2)}) async-start(bf16[8,384,256]{2,1,0:T(8,128)(2,1)} %broadcast_in_dim.2), calls=%async_computation | async-start | bytes 3145728 | tf_op jit(solution)/shard_map/all_to_all | solution.py:24
  15.3 0.0 copy-done.3
  15.3 0.0 copy-done.4
  15.3 0.0 copy-done.5
  15.3 0.0 copy-done.6
  15.4 74.2 %all-gather = bf16[512,256]{1,0:T(8,128)(2,1)S(1)} all-gather(bf16[64,256]{1,0:T(8,128)(2,1)S(1)} %pad_maximum_fusion.2), channel_id=2, replica_groups=mesh['gp'=1,'pair'=2,'fa'=8,'fb'=4,'tx'=4,'tc'=2] {'fa'}, dimensions={0}, use_global_device_ids=true | all-gather | bytes 294912 | tf_op jit(solution)/shard_map/all_gather | solution.py:110
  89.5 0.1 fusion.46
  89.6 24.1 %all_gather.23 = bf16[8,256,128]{2,1,0:T(8,128)(2,1)} all-gather(bf16[8,64,128]{2,1,0:T(8,128)(2,1)S(1)} %get-tuple-element.26), channel_id=1, replica_groups=mesh['gp'=1,'pair'=2,'fa'=8,'fb'=4,'tx'=4,'tc'=2] {'fb'}, dimensions={1}, use_global_device_ids=true | all-gather | bytes 655360 | tf_op jit(solution)/shard_map/all_gather | solution.py:92
  113.7 1.9 collective-permute-start
  115.7 20.4 %all_gather.24 = bf16[8,256,128]{2,1,0:T(8,128)(2,1)S(1)} all-gather(bf16[8,64,128]{2,1,0:T(8,128)(2,1)S(1)} %get-tuple-element.25), channel_id=1, replica_groups=mesh['gp'=1,'pair'=2,'fa'=8,'fb'=4,'tx'=4,'tc'=2] {'fb'}, dimensions={1}, use_global_device_ids=true | all-gather | bytes 655360 | tf_op jit(solution)/shard_map/all_gather | solution.py:92
  136.1 4.1 %collective-permute-start.1 = (bf16[2048,128]{1,0:T(8,128)(2,1)S(1)}, bf16[2048,128]{1,0:T(8,128)(2,1)S(1)}, u32[]{:S(2)}, u32[]{:S(2)}) collective-permute-start(bf16[2048,128]{1,0:T(8,128)(2,1)S(1)} %bitcast.110), channel_id=1, source_target_pairs={{0,256},{256,0},{1,257},{257,1},{2,258},{258,2},{3,259},{259,3},{4... | collective-permute-start | bytes 1572872 | tf_op jit(solution)/shard_map/ppermute | solution.py:30
  140.1 0.0 copy-done.2
  140.1 0.1 pad_add_fusion.where
  140.2 0.0 all-to-all-done
  140.2 0.3 convert_bitcast_fusion
  140.5 0.4 copy.15
  140.9 0.4 fusion.3
  141.3 0.3 multiply_convert_fusion.normed
  141.6 1.7 fusion.23
  143.3 0.0 copy-start
  143.3 0.0 collective-permute-done
  143.3 0.6 fusion.27.product
  143.9 3.3 %collective-permute-done.1.late_b = bf16[2048,128]{1,0:T(8,128)(2,1)S(1)} collective-permute-done((bf16[2048,128]{1,0:T(8,128)(2,1)S(1)}, bf16[2048,128]{1,0:T(8,128)(2,1)S(1)}, u32[]{:S(2)}, u32[]{:S(2)}) %collective-permute-start.1) | collective-permute-done | bytes 524320 | tf_op jit(solution)/shard_map/ppermute | solution.py:30
  147.3 2.4 %mixer_terms.1 = (f32[4,384,256]{2,1,0:T(8,128)S(1)}, bf16[4,384,256]{2,1,0:T(8,128)(2,1)S(1)}) custom-call(s32[2]{0:T(128)S(1)} %pad_add_fusion.where, bf16[384,2048]{1,0:T(8,128)(2,1)S(1)} %multiply_convert_fusion.normed, f32[384,128]{1,0:T(8,128)S(1)} %fusion.27.product, f32[3,128]{1,0:T(4,128)S(1)} %copy-done, bf16[2048,128]{1,0:T(8,128)(2,1)S(1)} %bitcast.111, ...), custom_call_target="tpu_custom_call" | custom-call | flops 402653184 | bytes 7340032 | tf_op jit(solution)/shard_map/mixer_terms/pallas_call | solution.py:150
  149.6 2.0 collective-permute-start.2
  151.6 2.3 collective-permute-done.2
  153.8 0.2 add_convert_fusion
  154.0 0.0 copy-start.1
  154.1 16.9 %all_to_all.15 = bf16[4,384,256]{2,1,0:T(8,128)(2,1)S(1)} all-to-all(bf16[4,384,256]{2,1,0:T(8,128)(2,1)S(1)} %add_convert_fusion), channel_id=1, replica_groups=mesh['gp'=1,'pair'=2,'fa'=8,'fb'=4,'tx'=4,'tc'=2] {'tx'}, dimensions={0} | all-to-all | bytes 1572864 | tf_op jit(solution)/shard_map/all_to_all | solution.py:48
  170.9 0.1 convert_reduce_fusion.1
  171.1 14.4 %all-gather.1 = bf16[1536,256]{1,0:T(8,128)(2,1)S(1)} all-gather(bf16[384,256]{1,0:T(8,128)(2,1)S(1)} %add_convert_fusion.2), channel_id=3, replica_groups=mesh['gp'=1,'pair'=2,'fa'=8,'fb'=4,'tx'=4,'tc'=2] {'tx'}, dimensions={0}, use_global_device_ids=true | all-gather | bytes 983040 | tf_op jit(solution)/shard_map/all_gather | solution.py:39
  185.5 2.1 collective-permute-start.3
  187.7 0.0 copy-done.7
  187.7 2.0 collective-permute-done.3
  189.8 0.1 bitcast_dynamic-update-slice_fusion.6
  189.8 0.1 bitcast_dynamic-update-slice_fusion.5
  189.9 0.1 bitcast_dynamic-update-slice_fusion.4
  189.9 0.1 bitcast_dynamic-update-slice_fusion.3
  190.0 0.0 copy-start.10
  190.0 0.1 bitcast_dynamic-update-slice_fusion.2
  190.1 0.1 bitcast_dynamic-update-slice_fusion.1
  190.1 0.1 bitcast_dynamic-update-slice_fusion
  190.2 0.4 fusion
  190.6 5.3 %all-gather.4.cloned.1.call-done = bf16[3,2048,640]{2,1,0:T(8,128)(2,1)} async-done(((bf16[3,64,640]{2,1,0:T(8,128)(2,1)}), bf16[3,2048,640]{2,1,0:T(8,128)(2,1)}) %all-gather.4.cloned.1.call-update) | async-done | bytes 7864336 | tf_op jit(solution)/shard_map/all_gather | solution.py:185
  195.9 3.3 %fusion.15 = bf16[384,640]{1,0:T(8,128)(2,1)S(1)} fusion(bf16[3,2048,640]{2,1,0:T(8,128)(2,1)} %all-gather.4.cloned.1.call-done, bf16[384,2048]{1,0:T(8,128)(2,1)S(1)} %bitcast_dynamic-update-slice_fusion, f32[2048]{0:T(1024)S(1)} %copy-done.10, f32[384]{0:T(512)S(1)} %add_rsqrt_fusion), kind=kOutput, calls=%fused_computation.27 | convolution fusion | flops 1010024448 | bytes 4695552 | tf_op jit(solution)/shard_map/dot_general | solution.py:82
  199.2 0.1 convert.28
  199.3 0.6 copy-done.9
  199.9 1.5 fusion.16
  201.4 0.1 convert.29
  201.4 0.9 fusion.38
  202.3 1.4 fusion.6
  203.7 0.1 fusion.42
  203.9 0.1 pad_maximum_fusion
  204.0 2.0 collective-permute-start.4
  205.9 0.2 select_bitcast_fusion.3
  206.2 2.0 collective-permute-done.4
  208.2 0.2 fusion.12
  208.4 15.5 %all_to_all.16 = bf16[4,384,256]{2,1,0:T(8,128)(2,1)S(1)} all-to-all(bf16[4,384,256]{2,1,0:T(8,128)(2,1)S(1)} %fusion.12), channel_id=1, replica_groups=mesh['gp'=1,'pair'=2,'fa'=8,'fb'=4,'tx'=4,'tc'=2] {'tx'}, dimensions={0} | all-to-all | bytes 1572864 | tf_op jit(solution)/shard_map/all_to_all | solution.py:48
  223.9 0.1 convert_reduce_fusion
  224.0 0.7 add_convert_fusion.1
  (21 shorter events, 0.2 us)
Async XLA Ops:
  6.5 189.3 %all-gather.4.cloned.1.call-start = ((), (), s32[]{:S(2)}) async-start(), calls=%async_computation.3 | async-start | bytes 8110080 | tf_op jit(solution)/shard_map/all_gather | solution.py:185
  10.6 4.8 %copy-start.3 = (bf16[64,128]{1,0:T(8,128)(2,1)S(1)}, bf16[64,128]{1,0:T(8,128)(2,1)}, u32[]{:S(2)}) copy-start(bf16[64,128]{1,0:T(8,128)(2,1)} %param.16) | copy-start | bytes 49156
  10.6 4.8 %copy-start.4 = (bf16[128,64]{0,1:T(8,128)(2,1)S(1)}, bf16[128,64]{0,1:T(8,128)(2,1)}, u32[]{:S(2)}) copy-start(bf16[128,64]{0,1:T(8,128)(2,1)} %param.19) | copy-start | bytes 49156
  10.6 4.8 %copy-start.5 = (bf16[64,128]{1,0:T(8,128)(2,1)S(1)}, bf16[64,128]{1,0:T(8,128)(2,1)}, u32[]{:S(2)}) copy-start(bf16[64,128]{1,0:T(8,128)(2,1)} %param.15) | copy-start | bytes 49156
  10.6 4.8 %copy-start.6 = (bf16[64,128]{1,0:T(8,128)(2,1)S(1)}, bf16[64,128]{1,0:T(8,128)(2,1)}, u32[]{:S(2)}) copy-start(bf16[64,128]{1,0:T(8,128)(2,1)} %param.17) | copy-start | bytes 49156
  10.6 129.6 %all-to-all-start = ((bf16[8,384,256]{2,1,0:T(8,128)(2,1)}), bf16[8,384,256]{2,1,0:T(8,128)(2,1)S(1)}, u32[]{:S(2)}, u32[]{:S(2)}) async-start(bf16[8,384,256]{2,1,0:T(8,128)(2,1)} %broadcast_in_dim.2), calls=%async_computation | async-start | bytes 3145728 | tf_op jit(solution)/shard_map/all_to_all | solution.py:24
  15.3 124.8 %copy-start.2 = (f32[2048]{0:T(1024)S(1)}, f32[2048]{0:T(1024)}, u32[]{:S(2)}) copy-start(f32[2048]{0:T(1024)} %param.14) | copy-start | bytes 24580
  113.7 29.6 %collective-permute-start = (bf16[2048,128]{1,0:T(8,128)(2,1)}, bf16[2048,128]{1,0:T(8,128)(2,1)S(1)}, u32[]{:S(2)}, u32[]{:S(2)}) collective-permute-start(bf16[2048,128]{1,0:T(8,128)(2,1)} %bitcast.7), channel_id=1, source_target_pairs={{0,256},{256,0},{1,257},{257,1},{2,258},{258,2},{3,259},{259,3},{4... | collective-permute-start | bytes 1572872 | tf_op jit(solution)/shard_map/ppermute | solution.py:30
  136.1 11.2 %collective-permute-start.1 = (bf16[2048,128]{1,0:T(8,128)(2,1)S(1)}, bf16[2048,128]{1,0:T(8,128)(2,1)S(1)}, u32[]{:S(2)}, u32[]{:S(2)}) collective-permute-start(bf16[2048,128]{1,0:T(8,128)(2,1)S(1)} %bitcast.110), channel_id=1, source_target_pairs={{0,256},{256,0},{1,257},{257,1},{2,258},{258,2},{3,259},{259,3},{4... | collective-permute-start | bytes 1572872 | tf_op jit(solution)/shard_map/ppermute | solution.py:30
  143.3 4.0 %copy-start = (f32[3,128]{1,0:T(4,128)S(1)}, f32[3,128]{1,0:T(4,128)}, u32[]{:S(2)}) copy-start(f32[3,128]{1,0:T(4,128)} %taps.1) | copy-start | bytes 4612
  149.6 4.2 %collective-permute-start.2 = (bf16[4,384,256]{2,1,0:T(8,128)(2,1)S(1)}, bf16[4,384,256]{2,1,0:T(8,128)(2,1)S(1)}, u32[]{:S(2)}, u32[]{:S(2)}) collective-permute-start(bf16[4,384,256]{2,1,0:T(8,128)(2,1)S(1)} %get-tuple-element.8), channel_id=1, source_target_pairs={{0,1},{1,0},{2,3},{3,2},{4,5},{5,4},{6,7},{7,6},{8,9},{9,8},{10,11... | collective-permute-start | bytes 2359304 | tf_op jit(solution)/shard_map/ppermute | solution.py:30
  154.0 17.0 %copy-start.1 = (bf16[384,256]{1,0:T(8,128)(2,1)S(1)}, bf16[384,256]{1,0:T(8,128)(2,1)}, u32[]{:S(2)}) copy-start(bf16[384,256]{1,0:T(8,128)(2,1)} %param.13) | copy-start | bytes 589828
  170.9 16.7 %copy-start.8 = (f32[2,640]{1,0:T(2,128)S(1)}, f32[2,640]{1,0:T(2,128)}, u32[]{:S(2)}) copy-start(f32[2,640]{1,0:T(2,128)} %param.24) | copy-start | bytes 15364
  170.9 16.8 %copy-start.7 = (f32[2,3,640]{2,0,1:T(2,128)S(1)}, f32[2,3,640]{2,0,1:T(2,128)}, u32[]{:S(2)}) copy-start(f32[2,3,640]{2,0,1:T(2,128)} %param.23) | copy-start | bytes 46084
  185.5 4.2 %collective-permute-start.3 = (bf16[4,384,256]{2,1,0:T(8,128)(2,1)S(1)}, bf16[4,384,256]{2,1,0:T(8,128)(2,1)S(1)}, u32[]{:S(2)}, u32[]{:S(2)}) collective-permute-start(bf16[4,384,256]{2,1,0:T(8,128)(2,1)S(1)} %bitcast.113), channel_id=1, source_target_pairs={{0,1},{1,0},{2,3},{3,2},{4,5},{5,4},{6,7},{7,6},{8,9},{9,8},{10,11... | collective-permute-start | bytes 2359304 | tf_op jit(solution)/shard_map/ppermute | solution.py:30
  190.0 5.9 %copy-start.10 = (f32[2048]{0:T(1024)S(1)}, f32[2048]{0:T(1024)}, u32[]{:S(2)}) copy-start(f32[2048]{0:T(1024)} %param.20) | copy-start | bytes 24580
  195.9 4.0 %copy-start.9 = (bf16[3,2048,640]{2,1,0:T(8,128)(2,1)S(1)}, bf16[3,2048,640]{2,1,0:T(8,128)(2,1)}, u32[]{:S(2)}) copy-start(bf16[3,2048,640]{2,1,0:T(8,128)(2,1)} %all-gather.4.cloned.1.call-done) | copy-start | bytes 23592964
  204.0 4.2 %collective-permute-start.4 = (bf16[4,384,256]{2,1,0:T(8,128)(2,1)S(1)}, bf16[4,384,256]{2,1,0:T(8,128)(2,1)S(1)}, u32[]{:S(2)}, u32[]{:S(2)}) collective-permute-start(bf16[4,384,256]{2,1,0:T(8,128)(2,1)S(1)} %pad_maximum_fusion), channel_id=1, source_target_pairs={{0,1},{1,0},{2,3},{3,2},{4,5},{5,4},{6,7},{7,6},{8,9},{9,8},{10,11... | collective-permute-start | bytes 2359304 | tf_op jit(solution)/shard_map/ppermute | solution.py:30
Sparse Core Ops, SparseCore 0:
  9.4 186.3 all-gather.3

commit v5 on v4

--- a/solution.py
+++ b/solution.py
@@ -47,16 +47,6 @@
     pairs = (keep + received.astype(jnp.float32)).astype(jnp.bfloat16)
     parts = lax.all_to_all(pairs, "tx", 0, 0, tiled=True)
     return jnp.sum(parts.astype(jnp.float32), axis=0)
-
-
-def sent_and_summed(terms):
-    chips = lax.axis_size("tx")
-    width = terms.shape[1] // (chips * CORES)
-    blocks = [terms[:, k * width : (k + 1) * width] for k in range(chips * CORES)]
-    chosen = [by_core(*blocks[k : k + CORES]) for k in range(0, chips * CORES, CORES)]
-    keep = jnp.stack([pair[0] for pair in chosen])
-    send = jnp.stack([pair[1] for pair in chosen])
-    return pairs_and_summed(keep, send.astype(jnp.bfloat16))
 
 
 def conv_positions(values, taps):
@@ -165,6 +155,33 @@
     )(where, normed, product, taps, late_a, late_b)
 
 
+def down_body(side, hidden, weights, out):
+    chips, _, share = out.shape
+    for chip in range(chips):
+        piece = pl.ds(pl.multiple_of((CORES * chip + side[0]) * share, share), share)
+        out[chip] = dot_t(hidden[...], weights[weights.shape[0] - 1, piece, :]).astype(out.dtype)
+
+
+def down_terms(hidden, weights, side, dtype):
+    rows, width = hidden.shape
+    features = weights.shape[1]
+    chips = lax.axis_size("tx")
+    vmem = pl.BlockSpec(memory_space=pltpu.VMEM)
+    return pl.pallas_call(
+        down_body,
+        in_specs=[pl.BlockSpec(memory_space=pltpu.SMEM), vmem, vmem],
+        out_specs=vmem,
+        out_shape=jax.ShapeDtypeStruct((chips, rows, features // (chips * CORES)), dtype),
+        compiler_params=pltpu.CompilerParams(vmem_limit_bytes=24 * 1024 * 1024),
+        cost_estimate=pl.CostEstimate(
+            flops=rows * features * width,
+            bytes_accessed=features * width + 3 * rows * features,
+            transcendentals=0,
+        ),
+        name="down_terms",
+    )(side.astype(jnp.int32).reshape(1), hidden, weights)
+
+
 def on_device(
     tokens,
     mix_gain,
@@ -182,7 +199,7 @@
     paired,
 ):
     shards = jnp.stack((w_gate, w_value, w_down.T))
-    gate_full, value_full, down_t = lax.all_gather(shards, FS, axis=1, tiled=True)
+    ffn_full = lax.all_gather(shards, FS, axis=1, tiled=True)
     whole = gathered_copies(tokens, TP)
     early_a, early_b, late_a, late_b = mixer_weights(
         w_signal, w_outer_gate, w_inner_gate, w_mix_out.T, paired
@@ -195,12 +212,15 @@
     resid = (tokens.astype(jnp.float32) + mix_sum).astype(jnp.bfloat16)
     whole_ffn = gathered_features(resid)
     normed_ffn = rms_norm(whole_ffn, ffn_gain)
-    gate = rounded(dot(normed_ffn, gate_full))
-    value = rounded(dot(normed_ffn, value_full))
+    gate = rounded(dot(normed_ffn, ffn_full[0]))
+    value = rounded(dot(normed_ffn, ffn_full[1]))
     gate_conv = conv_positions(gate, up_taps[0]) + up_bias[0]
     value_conv = conv_positions(value, up_taps[1]) + up_bias[1]
     hidden = (jax.nn.silu(gate_conv) * value_conv).astype(jnp.bfloat16)
-    ffn_sum = sent_and_summed(dot_t(hidden, down_t))
+    core = lax.axis_index("tc")
+    send = down_terms(hidden, ffn_full, 1 - core, jnp.bfloat16)
+    keep = down_terms(hidden, ffn_full, core, jnp.float32)
+    ffn_sum = pairs_and_summed(keep, send)
     return (resid.astype(jnp.float32) + ffn_sum).astype(jnp.bfloat16)
 
 

time: 232 us -> 232 us (level)
  no operation moved by 1% of the time
where the time goes in v5:
time: 232 us; the launch traced here: 231 us
  blocking collectives  166 us (72%)
  starting transfers between devices  16.7 us (7%)
  waiting for transfers between devices  14.4 us (6%)
  between operations  13.8 us (6%)
  matrix products  6.99 us (3%)
  other arithmetic  6.04 us (3%)
  Pallas kernels  3.97 us (2%)
  local copies, waits for them, and re-layouts  3.41 us (1%)
    all_gather x1, blocking collectives, mixer_weights(): far = lax.all_gather(side_by_side((early, late)), 'fa', axis=0)  74.2 us
    all_gather x2, blocking collectives, near_gather(): wide = lax.all_gather(far, 'fb', axis=1, tiled=True)  44.4 us
    all_to_all x2, blocking collectives, pairs_and_summed(): parts = lax.all_to_all(pairs, 'tx', 0, 0, tiled=True)  32.7 us
    all_gather x1, blocking collectives, gathered_features(): own = lax.all_gather(value, 'tx', axis=0)  14.3 us
    ppermute x5, starting transfers between devices, swapped(): return lax.ppermute(value, axis, [(0, 1), (1, 0)])  12 us
    ppermute x5, waiting for transfers between devices, swapped(): return lax.ppermute(value, axis, [(0, 1), (1, 0)])  9.02 us
    dot_general x4, matrix products, dot(): return jnp.dot(left, right, preferred_element_type=jnp.float32)  6.99 us
    all_gather x1, waiting for transfers between devices, on_device(): ffn_full = lax.all_gather(shards, FS, axis=1, tiled=True)  5.36 us
  transfers between devices with their start and end apart: 7, of which 5 were waited for; matrix products, arithmetic and copies ran while one was open for 3% of the time, Pallas kernels for 1%

profile of v5, /device:TPU:40, one launch (start us, length us, event | category | flops | bytes accessed | tf_op | source)
XLA Modules:
  0.0 231.0 jit_solution(12011545046788538532)
XLA Ops:
  6.5 0.0 all-gather.4.cloned.1.call-start
  6.6 1.7 pad_maximum_fusion
  8.2 0.1 all-gather.4.cloned.1.call-update
  8.3 2.3 broadcast_in_dim.2
  10.6 4.7 %all-to-all-start = ((bf16[8,384,256]{2,1,0:T(8,128)(2,1)}), bf16[8,384,256]{2,1,0:T(8,128)(2,1)S(1)}, u32[]{:S(2)}, u32[]{:S(2)}) async-start(bf16[8,384,256]{2,1,0:T(8,128)(2,1)} %broadcast_in_dim.2), calls=%async_computation | async-start | bytes 3145728 | tf_op jit(solution)/shard_map/all_to_all | solution.py:24
  15.3 0.0 copy-done.4
  15.3 0.0 copy-done.5
  15.3 0.0 copy-done.6
  15.3 0.0 copy-done.7
  15.4 74.2 %all-gather = bf16[512,256]{1,0:T(8,128)(2,1)S(1)} all-gather(bf16[64,256]{1,0:T(8,128)(2,1)S(1)} %pad_maximum_fusion.1), channel_id=2, replica_groups=mesh['gp'=1,'pair'=2,'fa'=8,'fb'=4,'tx'=4,'tc'=2] {'fa'}, dimensions={0}, use_global_device_ids=true | all-gather | bytes 294912 | tf_op jit(solution)/shard_map/all_gather | solution.py:100
  89.5 0.1 fusion.38
  89.6 24.1 %all_gather.23 = bf16[8,256,128]{2,1,0:T(8,128)(2,1)} all-gather(bf16[8,64,128]{2,1,0:T(8,128)(2,1)S(1)} %get-tuple-element.18), channel_id=1, replica_groups=mesh['gp'=1,'pair'=2,'fa'=8,'fb'=4,'tx'=4,'tc'=2] {'fb'}, dimensions={1}, use_global_device_ids=true | all-gather | bytes 655360 | tf_op jit(solution)/shard_map/all_gather | solution.py:82
  113.7 1.9 collective-permute-start
  115.7 20.3 %all_gather.24 = bf16[8,256,128]{2,1,0:T(8,128)(2,1)S(1)} all-gather(bf16[8,64,128]{2,1,0:T(8,128)(2,1)S(1)} %get-tuple-element.17), channel_id=1, replica_groups=mesh['gp'=1,'pair'=2,'fa'=8,'fb'=4,'tx'=4,'tc'=2] {'fb'}, dimensions={1}, use_global_device_ids=true | all-gather | bytes 655360 | tf_op jit(solution)/shard_map/all_gather | solution.py:82
  136.0 4.0 %collective-permute-start.1 = (bf16[2048,128]{1,0:T(8,128)(2,1)S(1)}, bf16[2048,128]{1,0:T(8,128)(2,1)S(1)}, u32[]{:S(2)}, u32[]{:S(2)}) collective-permute-start(bf16[2048,128]{1,0:T(8,128)(2,1)S(1)} %bitcast.100), channel_id=1, source_target_pairs={{0,256},{256,0},{1,257},{257,1},{2,258},{258,2},{3,259},{259,3},{4... | collective-permute-start | bytes 1572872 | tf_op jit(solution)/shard_map/ppermute | solution.py:30
  140.0 0.1 pad_add_fusion.where
  140.1 0.0 all-to-all-done
  140.1 0.3 convert_bitcast_fusion
  140.4 0.4 copy.15
  140.8 0.4 fusion.3
  141.2 0.3 multiply_convert_fusion.normed
  141.5 1.7 fusion.21
  143.2 0.0 copy-start.1
  143.2 0.0 collective-permute-done
  143.2 0.6 fusion.25.product
  143.8 3.4 %collective-permute-done.1.late_b = bf16[2048,128]{1,0:T(8,128)(2,1)S(1)} collective-permute-done((bf16[2048,128]{1,0:T(8,128)(2,1)S(1)}, bf16[2048,128]{1,0:T(8,128)(2,1)S(1)}, u32[]{:S(2)}, u32[]{:S(2)}) %collective-permute-start.1) | collective-permute-done | bytes 524320 | tf_op jit(solution)/shard_map/ppermute | solution.py:30
  147.2 2.4 %mixer_terms.1 = (f32[4,384,256]{2,1,0:T(8,128)S(1)}, bf16[4,384,256]{2,1,0:T(8,128)(2,1)S(1)}) custom-call(s32[2]{0:T(128)S(1)} %pad_add_fusion.where, bf16[384,2048]{1,0:T(8,128)(2,1)S(1)} %multiply_convert_fusion.normed, f32[384,128]{1,0:T(8,128)S(1)} %fusion.25.product, f32[3,128]{1,0:T(4,128)S(1)} %copy-done.1, bf16[2048,128]{1,0:T(8,128)(2,1)S(1)} %bitcast.101, ...), custom_call_target="tpu_custom_call" | custom-call | flops 402653184 | bytes 7340032 | tf_op jit(solution)/shard_map/mixer_terms/pallas_call | solution.py:140
  149.5 2.0 collective-permute-start.2
  151.5 2.3 collective-permute-done.2
  153.7 0.2 add_convert_fusion.1
  154.0 0.0 copy-start.2
  154.0 17.0 %all_to_all.15 = bf16[4,384,256]{2,1,0:T(8,128)(2,1)S(1)} all-to-all(bf16[4,384,256]{2,1,0:T(8,128)(2,1)S(1)} %add_convert_fusion.1), channel_id=1, replica_groups=mesh['gp'=1,'pair'=2,'fa'=8,'fb'=4,'tx'=4,'tc'=2] {'tx'}, dimensions={0} | all-to-all | bytes 1572864 | tf_op jit(solution)/shard_map/all_to_all | solution.py:48
  171.0 0.1 convert_reduce_fusion.1
  171.1 0.0 copy-done.2
  171.1 14.3 %all-gather.1 = bf16[1536,256]{1,0:T(8,128)(2,1)S(1)} all-gather(bf16[384,256]{1,0:T(8,128)(2,1)S(1)} %add_convert_fusion.3), channel_id=3, replica_groups=mesh['gp'=1,'pair'=2,'fa'=8,'fb'=4,'tx'=4,'tc'=2] {'tx'}, dimensions={0}, use_global_device_ids=true | all-gather | bytes 983040 | tf_op jit(solution)/shard_map/all_gather | solution.py:39
  185.4 2.1 collective-permute-start.3
  187.6 0.0 copy-done.8
  187.7 2.0 collective-permute-done.3
  189.7 0.1 bitcast_dynamic-update-slice_fusion.6
  189.8 0.1 bitcast_dynamic-update-slice_fusion.5
  189.8 0.1 bitcast_dynamic-update-slice_fusion.4
  189.9 0.1 bitcast_dynamic-update-slice_fusion.3
  189.9 0.0 copy-start.10
  189.9 0.1 bitcast_dynamic-update-slice_fusion.2
  190.0 0.1 bitcast_dynamic-update-slice_fusion.1
  190.1 0.1 bitcast_dynamic-update-slice_fusion
  190.1 0.4 fusion
  190.5 5.4 %all-gather.4.cloned.1.call-done.weights = bf16[3,2048,640]{2,1,0:T(8,128)(2,1)} async-done(((bf16[3,64,640]{2,1,0:T(8,128)(2,1)}), bf16[3,2048,640]{2,1,0:T(8,128)(2,1)}) %all-gather.4.cloned.1.call-update) | async-done | bytes 7864336 | tf_op jit(solution)/shard_map/all_gather | solution.py:202
  195.9 3.3 %fusion.13 = bf16[384,640]{1,0:T(8,128)(2,1)S(1)} fusion(bf16[3,2048,640]{2,1,0:T(8,128)(2,1)} %all-gather.4.cloned.1.call-done.weights, bf16[384,2048]{1,0:T(8,128)(2,1)S(1)} %bitcast_dynamic-update-slice_fusion, f32[2048]{0:T(1024)S(1)} %copy-done.10, f32[384]{0:T(512)S(1)} %add_rsqrt_fusion), kind=kOutput, calls=%fused_computation.24 | convolution fusion | flops 1010024448 | bytes 4695552 | tf_op jit(solution)/shard_map/dot_general | solution.py:72
  199.2 0.1 convert.8
  199.3 0.6 copy-done
  199.9 1.4 fusion.14
  201.3 0.1 convert.9
  201.4 0.3 fusion.28
  201.7 0.3 fusion.32
  202.0 0.3 fusion.35.hidden
  202.3 0.8 down_terms.3
  203.1 2.0 collective-permute-start.4
  205.1 0.8 down_terms.2
  205.9 1.4 collective-permute-done.4
  207.3 0.2 add_convert_fusion
  207.6 15.8 %all_to_all.16 = bf16[4,384,256]{2,1,0:T(8,128)(2,1)S(1)} all-to-all(bf16[4,384,256]{2,1,0:T(8,128)(2,1)S(1)} %add_convert_fusion), channel_id=1, replica_groups=mesh['gp'=1,'pair'=2,'fa'=8,'fb'=4,'tx'=4,'tc'=2] {'tx'}, dimensions={0} | all-to-all | bytes 1572864 | tf_op jit(solution)/shard_map/all_to_all | solution.py:48
  223.3 0.1 convert_reduce_fusion
  223.4 0.7 add_convert_fusion.2
  (21 shorter events, 0.2 us)
Async XLA Ops:
  6.5 189.3 %all-gather.4.cloned.1.call-start = ((), (), s32[]{:S(2)}) async-start(), calls=%async_computation.3 | async-start | bytes 8110080 | tf_op jit(solution)/shard_map/all_gather | solution.py:202
  10.6 4.8 %copy-start.4 = (bf16[64,128]{1,0:T(8,128)(2,1)S(1)}, bf16[64,128]{1,0:T(8,128)(2,1)}, u32[]{:S(2)}) copy-start(bf16[64,128]{1,0:T(8,128)(2,1)} %param.16) | copy-start | bytes 49156
  10.6 4.8 %copy-start.5 = (bf16[128,64]{0,1:T(8,128)(2,1)S(1)}, bf16[128,64]{0,1:T(8,128)(2,1)}, u32[]{:S(2)}) copy-start(bf16[128,64]{0,1:T(8,128)(2,1)} %param.19) | copy-start | bytes 49156
  10.6 4.8 %copy-start.6 = (bf16[64,128]{1,0:T(8,128)(2,1)S(1)}, bf16[64,128]{1,0:T(8,128)(2,1)}, u32[]{:S(2)}) copy-start(bf16[64,128]{1,0:T(8,128)(2,1)} %param.15) | copy-start | bytes 49156
  10.6 4.8 %copy-start.7 = (bf16[64,128]{1,0:T(8,128)(2,1)S(1)}, bf16[64,128]{1,0:T(8,128)(2,1)}, u32[]{:S(2)}) copy-start(bf16[64,128]{1,0:T(8,128)(2,1)} %param.17) | copy-start | bytes 49156
  10.6 129.6 %all-to-all-start = ((bf16[8,384,256]{2,1,0:T(8,128)(2,1)}), bf16[8,384,256]{2,1,0:T(8,128)(2,1)S(1)}, u32[]{:S(2)}, u32[]{:S(2)}) async-start(bf16[8,384,256]{2,1,0:T(8,128)(2,1)} %broadcast_in_dim.2), calls=%async_computation | async-start | bytes 3145728 | tf_op jit(solution)/shard_map/all_to_all | solution.py:24
  15.3 124.7 %copy-start.3 = (f32[2048]{0:T(1024)S(1)}, f32[2048]{0:T(1024)}, u32[]{:S(2)}) copy-start(f32[2048]{0:T(1024)} %param.14) | copy-start | bytes 24580
  113.7 29.5 %collective-permute-start = (bf16[2048,128]{1,0:T(8,128)(2,1)}, bf16[2048,128]{1,0:T(8,128)(2,1)S(1)}, u32[]{:S(2)}, u32[]{:S(2)}) collective-permute-start(bf16[2048,128]{1,0:T(8,128)(2,1)} %bitcast.7), channel_id=1, source_target_pairs={{0,256},{256,0},{1,257},{257,1},{2,258},{258,2},{3,259},{259,3},{4... | collective-permute-start | bytes 1572872 | tf_op jit(solution)/shard_map/ppermute | solution.py:30
  136.0 11.2 %collective-permute-start.1 = (bf16[2048,128]{1,0:T(8,128)(2,1)S(1)}, bf16[2048,128]{1,0:T(8,128)(2,1)S(1)}, u32[]{:S(2)}, u32[]{:S(2)}) collective-permute-start(bf16[2048,128]{1,0:T(8,128)(2,1)S(1)} %bitcast.100), channel_id=1, source_target_pairs={{0,256},{256,0},{1,257},{257,1},{2,258},{258,2},{3,259},{259,3},{4... | collective-permute-start | bytes 1572872 | tf_op jit(solution)/shard_map/ppermute | solution.py:30
  143.2 4.0 %copy-start.1 = (f32[3,128]{1,0:T(4,128)S(1)}, f32[3,128]{1,0:T(4,128)}, u32[]{:S(2)}) copy-start(f32[3,128]{1,0:T(4,128)} %taps.1) | copy-start | bytes 4612
  149.5 4.2 %collective-permute-start.2 = (bf16[4,384,256]{2,1,0:T(8,128)(2,1)S(1)}, bf16[4,384,256]{2,1,0:T(8,128)(2,1)S(1)}, u32[]{:S(2)}, u32[]{:S(2)}) collective-permute-start(bf16[4,384,256]{2,1,0:T(8,128)(2,1)S(1)} %get-tuple-element.8), channel_id=1, source_target_pairs={{0,1},{1,0},{2,3},{3,2},{4,5},{5,4},{6,7},{7,6},{8,9},{9,8},{10,11... | collective-permute-start | bytes 2359304 | tf_op jit(solution)/shard_map/ppermute | solution.py:30
  154.0 17.1 %copy-start.2 = (bf16[384,256]{1,0:T(8,128)(2,1)S(1)}, bf16[384,256]{1,0:T(8,128)(2,1)}, u32[]{:S(2)}) copy-start(bf16[384,256]{1,0:T(8,128)(2,1)} %param.13) | copy-start | bytes 589828
  171.0 16.6 %copy-start.9 = (f32[2,640]{1,0:T(2,128)S(1)}, f32[2,640]{1,0:T(2,128)}, u32[]{:S(2)}) copy-start(f32[2,640]{1,0:T(2,128)} %param.24) | copy-start | bytes 15364
  171.0 16.7 %copy-start.8 = (f32[2,3,640]{2,0,1:T(2,128)S(1)}, f32[2,3,640]{2,0,1:T(2,128)}, u32[]{:S(2)}) copy-start(f32[2,3,640]{2,0,1:T(2,128)} %param.23) | copy-start | bytes 46084
  185.4 4.2 %collective-permute-start.3 = (bf16[4,384,256]{2,1,0:T(8,128)(2,1)S(1)}, bf16[4,384,256]{2,1,0:T(8,128)(2,1)S(1)}, u32[]{:S(2)}, u32[]{:S(2)}) collective-permute-start(bf16[4,384,256]{2,1,0:T(8,128)(2,1)S(1)} %bitcast.103), channel_id=1, source_target_pairs={{0,1},{1,0},{2,3},{3,2},{4,5},{5,4},{6,7},{7,6},{8,9},{9,8},{10,11... | collective-permute-start | bytes 2359304 | tf_op jit(solution)/shard_map/ppermute | solution.py:30
  189.9 5.9 %copy-start.10 = (f32[2048]{0:T(1024)S(1)}, f32[2048]{0:T(1024)}, u32[]{:S(2)}) copy-start(f32[2048]{0:T(1024)} %param.20) | copy-start | bytes 24580
  195.9 4.0 %copy-start = (bf16[3,2048,640]{2,1,0:T(8,128)(2,1)S(1)}, bf16[3,2048,640]{2,1,0:T(8,128)(2,1)}, u32[]{:S(2)}) copy-start(bf16[3,2048,640]{2,1,0:T(8,128)(2,1)} %all-gather.4.cloned.1.call-done.weights) | copy-start | bytes 23592964
  203.1 4.2 %collective-permute-start.4 = (bf16[4,384,256]{2,1,0:T(8,128)(2,1)S(1)}, bf16[4,384,256]{2,1,0:T(8,128)(2,1)S(1)}, u32[]{:S(2)}, u32[]{:S(2)}) collective-permute-start(bf16[4,384,256]{2,1,0:T(8,128)(2,1)S(1)} %down_terms.3), channel_id=1, source_target_pairs={{0,1},{1,0},{2,3},{3,2},{4,5},{5,4},{6,7},{7,6},{8,9},{9,8},{10,11... | collective-permute-start | bytes 2359304 | tf_op jit(solution)/shard_map/ppermute | solution.py:30
Sparse Core Ops, SparseCore 0:
  9.4 186.3 all-gather.3

commit v6 on v5

--- a/solution.py
+++ b/solution.py
@@ -8,7 +8,7 @@
 
 SEQS_DEV = 2
 CORES = 2
-NEAR = 4
+NEAR = 2
 
 TP = ("tx", "tc")
 FS = ("fa", "fb")

time: 232 us -> 228 us (0.983)
  blocking collectives: 166 us -> 155 us
  local copies, waits for them, and re-layouts: 3.41 us -> 8.54 us
  other arithmetic: 6.04 us -> 10.1 us
  waiting for transfers between devices: 14.4 us -> 11.4 us
    all_gather x2, blocking collectives: 44.4 us -> 25.2 us  [near_gather(): wide = lax.all_gather(far, 'fb', axis=1, tiled=True)]
    all_gather x1, blocking collectives: 74.2 us -> 80.8 us  [mixer_weights(): far = lax.all_gather(side_by_side((early, late)), 'fa', axis=0)]
    ppermute x5, waiting for transfers between devices: 9.02 us -> 5.66 us  [swapped(): return lax.ppermute(value, axis, [(0, 1), (1, 0)])]
    convert_element_type x1, local copies, waits for them, and re-layouts: 0.36 us -> 3.61 us  [rms_norm(): values = stream.astype(jnp.float32)]
  transfers between devices with their start and end apart: 7 -> 7, of which waited for: 5 -> 4; matrix products, arithmetic and copies ran while one was open for 3% -> 7% of each run, Pallas kernels for 1% -> 1%
where the time goes in v6:
time: 228 us; the launch traced here: 227 us
  blocking collectives  155 us (68%)
  starting transfers between devices  17.1 us (8%)
  between operations  13.8 us (6%)
  waiting for transfers between devices  11.4 us (5%)
  other arithmetic  10.1 us (4%)
  local copies, waits for them, and re-layouts  8.54 us (4%)
  matrix products  7 us (3%)
  Pallas kernels  3.97 us (2%)
    all_gather x1, blocking collectives, mixer_weights(): far = lax.all_gather(side_by_side((early, late)), 'fa', axis=0)  80.8 us
    all_to_all x2, blocking collectives, pairs_and_summed(): parts = lax.all_to_all(pairs, 'tx', 0, 0, tiled=True)  34.8 us
    all_gather x2, blocking collectives, near_gather(): wide = lax.all_gather(far, 'fb', axis=1, tiled=True)  25.2 us
    all_gather x1, blocking collectives, gathered_features(): own = lax.all_gather(value, 'tx', axis=0)  14.2 us
    ppermute x5, starting transfers between devices, swapped(): return lax.ppermute(value, axis, [(0, 1), (1, 0)])  12.4 us
    dot_general x4, matrix products, dot(): return jnp.dot(left, right, preferred_element_type=jnp.float32)  7 us
    all_gather x1, waiting for transfers between devices, on_device(): ffn_full = lax.all_gather(shards, FS, axis=1, tiled=True)  5.73 us
    ppermute x5, waiting for transfers between devices, swapped(): return lax.ppermute(value, axis, [(0, 1), (1, 0)])  5.66 us
  transfers between devices with their start and end apart: 7, of which 4 were waited for; matrix products, arithmetic and copies ran while one was open for 7% of the time, Pallas kernels for 1%

profile of v6, /device:TPU:40, one launch (start us, length us, event | category | flops | bytes accessed | tf_op | source)
XLA Modules:
  0.0 227.1 jit_solution(4028822870161810508)
XLA Ops:
  6.5 0.0 all-gather.4.cloned.1.call-start
  6.6 1.7 pad_maximum_fusion
  8.3 0.1 all-gather.4.cloned.1.call-update
  8.3 2.2 broadcast_in_dim.2
  10.5 4.7 %all-to-all-start = ((bf16[8,384,256]{2,1,0:T(8,128)(2,1)}), bf16[8,384,256]{2,1,0:T(8,128)(2,1)}, u32[]{:S(2)}, u32[]{:S(2)}) async-start(bf16[8,384,256]{2,1,0:T(8,128)(2,1)} %broadcast_in_dim.2), calls=%async_computation | async-start | bytes 3145728 | tf_op jit(solution)/shard_map/all_to_all | solution.py:24
  15.3 0.0 copy-done.4
  15.3 0.0 copy-done.5
  15.3 0.0 copy-done.6
  15.3 0.0 copy-start.3
  15.3 80.8 %all-gather = bf16[1024,256]{1,0:T(8,128)(2,1)S(1)} all-gather(bf16[64,256]{1,0:T(8,128)(2,1)S(1)} %pad_maximum_fusion.1), channel_id=2, replica_groups=mesh['gp'=1,'pair'=2,'fa'=16,'fb'=2,'tx'=4,'tc'=2] {'fa'}, dimensions={0}, use_global_device_ids=true | all-gather | bytes 557056 | tf_op jit(solution)/shard_map/all_gather | solution.py:100
  96.2 0.1 fusion.22
  96.3 12.7 %all_gather.23 = bf16[16,128,128]{2,1,0:T(8,128)(2,1)S(1)} all-gather(bf16[16,64,128]{2,1,0:T(8,128)(2,1)S(1)} %get-tuple-element.18), channel_id=1, replica_groups=mesh['gp'=1,'pair'=2,'fa'=16,'fb'=2,'tx'=4,'tc'=2] {'fb'}, dimensions={1}, use_global_device_ids=true | all-gather | bytes 786432 | tf_op jit(solution)/shard_map/all_gather | solution.py:82
  109.0 1.9 collective-permute-start
  110.9 12.5 %all_gather.24 = bf16[16,128,128]{2,1,0:T(8,128)(2,1)S(1)} all-gather(bf16[16,64,128]{2,1,0:T(8,128)(2,1)S(1)} %get-tuple-element.17), channel_id=1, replica_groups=mesh['gp'=1,'pair'=2,'fa'=16,'fb'=2,'tx'=4,'tc'=2] {'fb'}, dimensions={1}, use_global_device_ids=true | all-gather | bytes 786432 | tf_op jit(solution)/shard_map/all_gather | solution.py:82
  123.5 4.4 %collective-permute-start.1 = (bf16[2048,128]{1,0:T(8,128)(2,1)S(1)}, bf16[2048,128]{1,0:T(8,128)(2,1)S(1)}, u32[]{:S(2)}, u32[]{:S(2)}) collective-permute-start(bf16[2048,128]{1,0:T(8,128)(2,1)S(1)} %bitcast.88), channel_id=1, source_target_pairs={{0,256},{256,0},{1,257},{257,1},{2,258},{258,2},{3,259},{259,3},{4... | collective-permute-start | bytes 1572872 | tf_op jit(solution)/shard_map/ppermute | solution.py:30
  127.9 0.1 pad_add_fusion.where
  128.0 0.0 all-to-all-done
  128.0 1.9 copy.15
  129.9 2.0 convert_element_type.107
  131.9 3.6 %copy.17 = f32[384,2048]{1,0:T(8,128)} copy(f32[384,2048]{0,1:T(8,128)} %bitcast.90) | data formatting | bytes 6291456 | tf_op jit(solution)/shard_map/convert_element_type | solution.py:66
  135.5 0.4 multiply_reduce_fusion
  135.9 2.2 multiply_convert_fusion.1.normed
  138.1 0.4 multiply_convert_fusion
  138.6 0.6 fusion.9
  139.2 0.0 copy-start.1
  139.2 0.0 collective-permute-done
  139.2 1.6 fusion.8.product
  140.8 0.0 collective-permute-done.1.late_b
  140.9 2.4 %mixer_terms.1 = (f32[4,384,256]{2,1,0:T(8,128)S(1)}, bf16[4,384,256]{2,1,0:T(8,128)(2,1)S(1)}) custom-call(s32[2]{0:T(128)S(1)} %pad_add_fusion.where, bf16[384,2048]{1,0:T(8,128)(2,1)S(1)} %multiply_convert_fusion.1.normed, f32[384,128]{1,0:T(8,128)S(1)} %fusion.8.product, f32[3,128]{1,0:T(4,128)S(1)} %copy-done.1, bf16[2048,128]{1,0:T(8,128)(2,1)S(1)} %bitcast.89, ...), custom_call_target="tpu_custom_call" | custom-call | flops 402653184 | bytes 7340032 | tf_op jit(solution)/shard_map/mixer_terms/pallas_call | solution.py:140
  143.2 2.0 collective-permute-start.2
  145.2 2.3 collective-permute-done.2
  147.4 0.2 add_convert_fusion.1
  147.7 0.0 copy-start.2
  147.7 17.9 %all_to_all.15 = bf16[4,384,256]{2,1,0:T(8,128)(2,1)S(1)} all-to-all(bf16[4,384,256]{2,1,0:T(8,128)(2,1)S(1)} %add_convert_fusion.1), channel_id=1, replica_groups=mesh['gp'=1,'pair'=2,'fa'=16,'fb'=2,'tx'=4,'tc'=2] {'tx'}, dimensions={0} | all-to-all | bytes 1572864 | tf_op jit(solution)/shard_map/all_to_all | solution.py:48
  165.5 0.1 convert_reduce_fusion.1
  165.7 14.2 %all-gather.1 = bf16[1536,256]{1,0:T(8,128)(2,1)S(1)} all-gather(bf16[384,256]{1,0:T(8,128)(2,1)S(1)} %add_convert_fusion.3), channel_id=3, replica_groups=mesh['gp'=1,'pair'=2,'fa'=16,'fb'=2,'tx'=4,'tc'=2] {'tx'}, dimensions={0}, use_global_device_ids=true | all-gather | bytes 983040 | tf_op jit(solution)/shard_map/all_gather | solution.py:39
  179.9 2.1 collective-permute-start.3
  182.2 2.0 collective-permute-done.3
  184.2 0.1 bitcast_dynamic-update-slice_fusion.6
  184.2 0.1 bitcast_dynamic-update-slice_fusion.5
  184.3 0.1 bitcast_dynamic-update-slice_fusion.4
  184.4 0.1 bitcast_dynamic-update-slice_fusion.3
  184.4 0.0 copy-start.10
  184.4 0.1 bitcast_dynamic-update-slice_fusion.2
  184.5 0.1 bitcast_dynamic-update-slice_fusion.1
  184.6 0.1 bitcast_dynamic-update-slice_fusion
  184.6 0.4 fusion
  185.0 5.7 %all-gather.4.cloned.1.call-done.weights = bf16[3,2048,640]{2,1,0:T(8,128)(2,1)} async-done(((bf16[3,64,640]{2,1,0:T(8,128)(2,1)}), bf16[3,2048,640]{2,1,0:T(8,128)(2,1)}) %all-gather.4.cloned.1.call-update) | async-done | bytes 7864336 | tf_op jit(solution)/shard_map/all_gather | solution.py:202
  190.7 3.3 %fusion.5 = bf16[384,640]{1,0:T(8,128)(2,1)S(1)} fusion(bf16[3,2048,640]{2,1,0:T(8,128)(2,1)} %all-gather.4.cloned.1.call-done.weights, bf16[384,2048]{1,0:T(8,128)(2,1)S(1)} %bitcast_dynamic-update-slice_fusion, f32[2048]{0:T(1024)S(1)} %copy-done.10, f32[384]{0:T(512)S(1)} %add_rsqrt_fusion), kind=kOutput, calls=%fused_computation.16 | convolution fusion | flops 1010024448 | bytes 4695552 | tf_op jit(solution)/shard_map/dot_general | solution.py:72
  194.1 0.1 convert.8
  194.1 0.6 copy-done
  194.8 1.4 fusion.6
  196.2 0.1 convert.9
  196.3 0.3 fusion.12
  196.6 0.3 fusion.16
  196.9 0.3 fusion.19.hidden
  197.2 0.8 down_terms.3
  198.0 2.0 collective-permute-start.4
  199.9 0.8 down_terms.2
  200.8 1.4 collective-permute-done.4
  202.2 0.2 add_convert_fusion
  202.4 17.0 %all_to_all.16 = bf16[4,384,256]{2,1,0:T(8,128)(2,1)S(1)} all-to-all(bf16[4,384,256]{2,1,0:T(8,128)(2,1)S(1)} %add_convert_fusion), channel_id=1, replica_groups=mesh['gp'=1,'pair'=2,'fa'=16,'fb'=2,'tx'=4,'tc'=2] {'tx'}, dimensions={0} | all-to-all | bytes 1572864 | tf_op jit(solution)/shard_map/all_to_all | solution.py:48
  219.4 0.1 convert_reduce_fusion
  219.5 0.7 add_convert_fusion.2
  (23 shorter events, 0.2 us)
Async XLA Ops:
  6.5 184.2 %all-gather.4.cloned.1.call-start = ((), (), s32[]{:S(2)}) async-start(), calls=%async_computation.3 | async-start | bytes 8110080 | tf_op jit(solution)/shard_map/all_gather | solution.py:202
  10.5 4.7 %copy-start.4 = (bf16[64,128]{1,0:T(8,128)(2,1)S(1)}, bf16[64,128]{1,0:T(8,128)(2,1)}, u32[]{:S(2)}) copy-start(bf16[64,128]{1,0:T(8,128)(2,1)} %param.16) | copy-start | bytes 49156
  10.5 4.7 %copy-start.5 = (bf16[128,64]{0,1:T(8,128)(2,1)S(1)}, bf16[128,64]{0,1:T(8,128)(2,1)}, u32[]{:S(2)}) copy-start(bf16[128,64]{0,1:T(8,128)(2,1)} %param.19) | copy-start | bytes 49156
  10.5 4.8 %copy-start.6 = (bf16[64,128]{1,0:T(8,128)(2,1)S(1)}, bf16[64,128]{1,0:T(8,128)(2,1)}, u32[]{:S(2)}) copy-start(bf16[64,128]{1,0:T(8,128)(2,1)} %param.15) | copy-start | bytes 49156
  10.5 4.8 %copy-start.7 = (bf16[64,128]{1,0:T(8,128)(2,1)S(1)}, bf16[64,128]{1,0:T(8,128)(2,1)}, u32[]{:S(2)}) copy-start(bf16[64,128]{1,0:T(8,128)(2,1)} %param.17) | copy-start | bytes 49156
  10.5 117.5 %all-to-all-start = ((bf16[8,384,256]{2,1,0:T(8,128)(2,1)}), bf16[8,384,256]{2,1,0:T(8,128)(2,1)}, u32[]{:S(2)}, u32[]{:S(2)}) async-start(bf16[8,384,256]{2,1,0:T(8,128)(2,1)} %broadcast_in_dim.2), calls=%async_computation | async-start | bytes 3145728 | tf_op jit(solution)/shard_map/all_to_all | solution.py:24
  15.3 112.6 %copy-start.3 = (f32[2048]{0:T(1024)S(1)}, f32[2048]{0:T(1024)}, u32[]{:S(2)}) copy-start(f32[2048]{0:T(1024)} %param.14) | copy-start | bytes 24580
  109.0 30.2 %collective-permute-start = (bf16[2048,128]{1,0:T(8,128)(2,1)S(1)}, bf16[2048,128]{1,0:T(8,128)(2,1)}, u32[]{:S(2)}, u32[]{:S(2)}) collective-permute-start(bf16[2048,128]{1,0:T(8,128)(2,1)S(1)} %bitcast.94), channel_id=1, source_target_pairs={{0,256},{256,0},{1,257},{257,1},{2,258},{258,2},{3,259},{259,3},{4... | collective-permute-start | bytes 1572872 | tf_op jit(solution)/shard_map/ppermute | solution.py:30
  123.5 17.4 %collective-permute-start.1 = (bf16[2048,128]{1,0:T(8,128)(2,1)S(1)}, bf16[2048,128]{1,0:T(8,128)(2,1)S(1)}, u32[]{:S(2)}, u32[]{:S(2)}) collective-permute-start(bf16[2048,128]{1,0:T(8,128)(2,1)S(1)} %bitcast.88), channel_id=1, source_target_pairs={{0,256},{256,0},{1,257},{257,1},{2,258},{258,2},{3,259},{259,3},{4... | collective-permute-start | bytes 1572872 | tf_op jit(solution)/shard_map/ppermute | solution.py:30
  139.2 1.7 copy-start.1
  143.2 4.2 %collective-permute-start.2 = (bf16[4,384,256]{2,1,0:T(8,128)(2,1)S(1)}, bf16[4,384,256]{2,1,0:T(8,128)(2,1)S(1)}, u32[]{:S(2)}, u32[]{:S(2)}) collective-permute-start(bf16[4,384,256]{2,1,0:T(8,128)(2,1)S(1)} %get-tuple-element.8), channel_id=1, source_target_pairs={{0,1},{1,0},{2,3},{3,2},{4,5},{5,4},{6,7},{7,6},{8,9},{9,8},{10,11... | collective-permute-start | bytes 2359304 | tf_op jit(solution)/shard_map/ppermute | solution.py:30
  147.7 18.0 %copy-start.2 = (bf16[384,256]{1,0:T(8,128)(2,1)S(1)}, bf16[384,256]{1,0:T(8,128)(2,1)}, u32[]{:S(2)}) copy-start(bf16[384,256]{1,0:T(8,128)(2,1)} %param.13) | copy-start | bytes 589828
  165.5 16.5 %copy-start.9 = (f32[2,640]{1,0:T(2,128)S(1)}, f32[2,640]{1,0:T(2,128)}, u32[]{:S(2)}) copy-start(f32[2,640]{1,0:T(2,128)} %param.24) | copy-start | bytes 15364
  165.5 16.6 %copy-start.8 = (f32[2,3,640]{2,0,1:T(2,128)S(1)}, f32[2,3,640]{2,0,1:T(2,128)}, u32[]{:S(2)}) copy-start(f32[2,3,640]{2,0,1:T(2,128)} %param.23) | copy-start | bytes 46084
  179.9 4.2 %collective-permute-start.3 = (bf16[4,384,256]{2,1,0:T(8,128)(2,1)S(1)}, bf16[4,384,256]{2,1,0:T(8,128)(2,1)S(1)}, u32[]{:S(2)}, u32[]{:S(2)}) collective-permute-start(bf16[4,384,256]{2,1,0:T(8,128)(2,1)S(1)} %bitcast.92), channel_id=1, source_target_pairs={{0,1},{1,0},{2,3},{3,2},{4,5},{5,4},{6,7},{7,6},{8,9},{9,8},{10,11... | collective-permute-start | bytes 2359304 | tf_op jit(solution)/shard_map/ppermute | solution.py:30
  184.4 6.3 %copy-start.10 = (f32[2048]{0:T(1024)S(1)}, f32[2048]{0:T(1024)}, u32[]{:S(2)}) copy-start(f32[2048]{0:T(1024)} %param.20) | copy-start | bytes 24580
  190.7 4.0 %copy-start = (bf16[3,2048,640]{2,1,0:T(8,128)(2,1)S(1)}, bf16[3,2048,640]{2,1,0:T(8,128)(2,1)}, u32[]{:S(2)}) copy-start(bf16[3,2048,640]{2,1,0:T(8,128)(2,1)} %all-gather.4.cloned.1.call-done.weights) | copy-start | bytes 23592964
  198.0 4.2 %collective-permute-start.4 = (bf16[4,384,256]{2,1,0:T(8,128)(2,1)S(1)}, bf16[4,384,256]{2,1,0:T(8,128)(2,1)S(1)}, u32[]{:S(2)}, u32[]{:S(2)}) collective-permute-start(bf16[4,384,256]{2,1,0:T(8,128)(2,1)S(1)} %down_terms.3), channel_id=1, source_target_pairs={{0,1},{1,0},{2,3},{3,2},{4,5},{5,4},{6,7},{7,6},{8,9},{9,8},{10,11... | collective-permute-start | bytes 2359304 | tf_op jit(solution)/shard_map/ppermute | solution.py:30
Sparse Core Ops, SparseCore 0:
  9.4 181.2 all-gather.3

commit v7 on v6

--- a/solution.py
+++ b/solution.py
@@ -211,7 +211,7 @@
     )
     resid = (tokens.astype(jnp.float32) + mix_sum).astype(jnp.bfloat16)
     whole_ffn = gathered_features(resid)
-    normed_ffn = rms_norm(whole_ffn, ffn_gain)
+    normed_ffn = lax.optimization_barrier(rms_norm(whole_ffn, ffn_gain))
     gate = rounded(dot(normed_ffn, ffn_full[0]))
     value = rounded(dot(normed_ffn, ffn_full[1]))
     gate_conv = conv_positions(gate, up_taps[0]) + up_bias[0]

time: 228 us -> 228 us (level)
  no operation moved by 1% of the time
where the time goes in v7:
time: 228 us; the launch traced here: 227 us
  blocking collectives  155 us (68%)
  starting transfers between devices  17.1 us (8%)
  between operations  13.8 us (6%)
  waiting for transfers between devices  10.9 us (5%)
  other arithmetic  10.5 us (5%)
  local copies, waits for them, and re-layouts  8.72 us (4%)
  matrix products  6.88 us (3%)
  Pallas kernels  3.97 us (2%)
    all_gather x1, blocking collectives, mixer_weights(): far = lax.all_gather(side_by_side((early, late)), 'fa', axis=0)  80.8 us
    all_to_all x2, blocking collectives, pairs_and_summed(): parts = lax.all_to_all(pairs, 'tx', 0, 0, tiled=True)  34.8 us
    all_gather x2, blocking collectives, near_gather(): wide = lax.all_gather(far, 'fb', axis=1, tiled=True)  25.2 us
    all_gather x1, blocking collectives, gathered_features(): own = lax.all_gather(value, 'tx', axis=0)  14.2 us
    ppermute x5, starting transfers between devices, swapped(): return lax.ppermute(value, axis, [(0, 1), (1, 0)])  12.4 us
    dot_general x4, matrix products, dot(): return jnp.dot(left, right, preferred_element_type=jnp.float32)  6.88 us
    ppermute x5, waiting for transfers between devices, swapped(): return lax.ppermute(value, axis, [(0, 1), (1, 0)])  5.66 us
    all_gather x1, waiting for transfers between devices, on_device(): ffn_full = lax.all_gather(shards, FS, axis=1, tiled=True)  5.18 us
  transfers between devices with their start and end apart: 7, of which 4 were waited for; matrix products, arithmetic and copies ran while one was open for 7% of the time, Pallas kernels for 1%

profile of v7, /device:TPU:40, one launch (start us, length us, event | category | flops | bytes accessed | tf_op | source)
XLA Modules:
  0.0 227.0 jit_solution(1823360934651922304)
XLA Ops:
  6.5 0.0 all-gather.4.cloned.1.call-start
  6.6 1.7 pad_maximum_fusion
  8.3 0.1 all-gather.4.cloned.1.call-update
  8.3 2.2 broadcast_in_dim.2
  10.5 4.7 %all-to-all-start = ((bf16[8,384,256]{2,1,0:T(8,128)(2,1)}), bf16[8,384,256]{2,1,0:T(8,128)(2,1)}, u32[]{:S(2)}, u32[]{:S(2)}) async-start(bf16[8,384,256]{2,1,0:T(8,128)(2,1)} %broadcast_in_dim.2), calls=%async_computation | async-start | bytes 3145728 | tf_op jit(solution)/shard_map/all_to_all | solution.py:24
  15.3 0.0 copy-start.3
  15.3 80.8 %all-gather = bf16[1024,256]{1,0:T(8,128)(2,1)S(1)} all-gather(bf16[64,256]{1,0:T(8,128)(2,1)S(1)} %pad_maximum_fusion.1), channel_id=2, replica_groups=mesh['gp'=1,'pair'=2,'fa'=16,'fb'=2,'tx'=4,'tc'=2] {'fa'}, dimensions={0}, use_global_device_ids=true | all-gather | bytes 557056 | tf_op jit(solution)/shard_map/all_gather | solution.py:100
  96.2 0.1 fusion.20
  96.3 12.7 %all_gather.23 = bf16[16,128,128]{2,1,0:T(8,128)(2,1)S(1)} all-gather(bf16[16,64,128]{2,1,0:T(8,128)(2,1)S(1)} %get-tuple-element.18), channel_id=1, replica_groups=mesh['gp'=1,'pair'=2,'fa'=16,'fb'=2,'tx'=4,'tc'=2] {'fb'}, dimensions={1}, use_global_device_ids=true | all-gather | bytes 786432 | tf_op jit(solution)/shard_map/all_gather | solution.py:82
  109.0 1.9 collective-permute-start
  110.9 12.5 %all_gather.24 = bf16[16,128,128]{2,1,0:T(8,128)(2,1)S(1)} all-gather(bf16[16,64,128]{2,1,0:T(8,128)(2,1)S(1)} %get-tuple-element.17), channel_id=1, replica_groups=mesh['gp'=1,'pair'=2,'fa'=16,'fb'=2,'tx'=4,'tc'=2] {'fb'}, dimensions={1}, use_global_device_ids=true | all-gather | bytes 786432 | tf_op jit(solution)/shard_map/all_gather | solution.py:82
  123.5 4.4 %collective-permute-start.1 = (bf16[2048,128]{1,0:T(8,128)(2,1)S(1)}, bf16[2048,128]{1,0:T(8,128)(2,1)S(1)}, u32[]{:S(2)}, u32[]{:S(2)}) collective-permute-start(bf16[2048,128]{1,0:T(8,128)(2,1)S(1)} %bitcast.90), channel_id=1, source_target_pairs={{0,256},{256,0},{1,257},{257,1},{2,258},{258,2},{3,259},{259,3},{4... | collective-permute-start | bytes 1572872 | tf_op jit(solution)/shard_map/ppermute | solution.py:30
  127.9 0.1 pad_add_fusion.where
  128.0 0.0 all-to-all-done
  128.0 1.9 copy.15
  129.9 2.0 convert_element_type.107
  131.9 3.6 %copy.17 = f32[384,2048]{1,0:T(8,128)} copy(f32[384,2048]{0,1:T(8,128)} %bitcast.92) | data formatting | bytes 6291456 | tf_op jit(solution)/shard_map/convert_element_type | solution.py:66
  135.5 0.4 multiply_reduce_fusion
  135.9 2.2 multiply_convert_fusion.1.normed
  138.1 0.4 multiply_convert_fusion
  138.6 0.6 fusion.9
  139.2 0.0 copy-start.1
  139.2 0.0 collective-permute-done
  139.2 1.6 fusion.8.product
  140.8 0.0 collective-permute-done.1.late_b
  140.9 2.4 %mixer_terms.1 = (f32[4,384,256]{2,1,0:T(8,128)S(1)}, bf16[4,384,256]{2,1,0:T(8,128)(2,1)S(1)}) custom-call(s32[2]{0:T(128)S(1)} %pad_add_fusion.where, bf16[384,2048]{1,0:T(8,128)(2,1)S(1)} %multiply_convert_fusion.1.normed, f32[384,128]{1,0:T(8,128)S(1)} %fusion.8.product, f32[3,128]{1,0:T(4,128)S(1)} %copy-done.1, bf16[2048,128]{1,0:T(8,128)(2,1)S(1)} %bitcast.91, ...), custom_call_target="tpu_custom_call" | custom-call | flops 402653184 | bytes 7340032 | tf_op jit(solution)/shard_map/mixer_terms/pallas_call | solution.py:140
  143.2 2.0 collective-permute-start.2
  145.2 2.3 collective-permute-done.2
  147.4 0.2 add_convert_fusion.1
  147.7 0.0 copy-start.2
  147.7 17.9 %all_to_all.15 = bf16[4,384,256]{2,1,0:T(8,128)(2,1)S(1)} all-to-all(bf16[4,384,256]{2,1,0:T(8,128)(2,1)S(1)} %add_convert_fusion.1), channel_id=1, replica_groups=mesh['gp'=1,'pair'=2,'fa'=16,'fb'=2,'tx'=4,'tc'=2] {'tx'}, dimensions={0} | all-to-all | bytes 1572864 | tf_op jit(solution)/shard_map/all_to_all | solution.py:48
  165.5 0.1 convert_reduce_fusion.1
  165.7 14.2 %all-gather.1 = bf16[1536,256]{1,0:T(8,128)(2,1)S(1)} all-gather(bf16[384,256]{1,0:T(8,128)(2,1)S(1)} %add_convert_fusion.3), channel_id=3, replica_groups=mesh['gp'=1,'pair'=2,'fa'=16,'fb'=2,'tx'=4,'tc'=2] {'tx'}, dimensions={0}, use_global_device_ids=true | all-gather | bytes 983040 | tf_op jit(solution)/shard_map/all_gather | solution.py:39
  179.9 2.1 collective-permute-start.3
  182.1 0.0 copy-done.8
  182.2 2.0 collective-permute-done.3
  184.2 0.1 bitcast_dynamic-update-slice_fusion.6
  184.2 0.1 bitcast_dynamic-update-slice_fusion.5
  184.3 0.1 bitcast_dynamic-update-slice_fusion.4
  184.4 0.1 bitcast_dynamic-update-slice_fusion.3
  184.4 0.0 copy-start.9
  184.4 0.1 bitcast_dynamic-update-slice_fusion.2
  184.5 0.1 bitcast_dynamic-update-slice_fusion.1
  184.6 0.1 bitcast_dynamic-update-slice_fusion
  184.6 0.4 fusion
  185.0 0.1 copy-done.9
  185.1 0.4 fusion.2
  185.6 5.2 %all-gather.4.cloned.1.call-done.weights = bf16[3,2048,640]{2,1,0:T(8,128)(2,1)} async-done(((bf16[3,64,640]{2,1,0:T(8,128)(2,1)}), bf16[3,2048,640]{2,1,0:T(8,128)(2,1)}) %all-gather.4.cloned.1.call-update) | async-done | bytes 7864336 | tf_op jit(solution)/shard_map/all_gather | solution.py:202
  190.7 3.3 %fusion.5 = bf16[384,640]{1,0:T(8,128)(2,1)S(1)} fusion(bf16[384,2048]{1,0:T(8,128)(2,1)S(1)} %fusion.2, bf16[3,2048,640]{2,1,0:T(8,128)(2,1)} %all-gather.4.cloned.1.call-done.weights), kind=kOutput, calls=%fused_computation.16 | convolution fusion | flops 1006878720 | bytes 4685824 | tf_op jit(solution)/shard_map/dot_general | solution.py:72
  194.0 0.1 convert.8
  194.1 0.7 copy-done
  194.8 1.4 fusion.6
  196.1 0.1 convert.9
  196.2 0.3 fusion.12
  196.5 0.3 fusion.16
  196.8 0.3 fusion.19.hidden
  197.1 0.8 down_terms.3
  197.9 2.0 collective-permute-start.4
  199.9 0.8 down_terms.2
  200.7 1.4 collective-permute-done.4
  202.1 0.2 add_convert_fusion
  202.4 17.0 %all_to_all.16 = bf16[4,384,256]{2,1,0:T(8,128)(2,1)S(1)} all-to-all(bf16[4,384,256]{2,1,0:T(8,128)(2,1)S(1)} %add_convert_fusion), channel_id=1, replica_groups=mesh['gp'=1,'pair'=2,'fa'=16,'fb'=2,'tx'=4,'tc'=2] {'tx'}, dimensions={0} | all-to-all | bytes 1572864 | tf_op jit(solution)/shard_map/all_to_all | solution.py:48
  219.4 0.1 convert_reduce_fusion
  219.5 0.7 add_convert_fusion.2
  (24 shorter events, 0.2 us)
Async XLA Ops:
  6.5 184.2 %all-gather.4.cloned.1.call-start = ((), (), s32[]{:S(2)}) async-start(), calls=%async_computation.3 | async-start | bytes 8110080 | tf_op jit(solution)/shard_map/all_gather | solution.py:202
  10.5 4.7 %copy-start.4 = (bf16[64,128]{1,0:T(8,128)(2,1)S(1)}, bf16[64,128]{1,0:T(8,128)(2,1)}, u32[]{:S(2)}) copy-start(bf16[64,128]{1,0:T(8,128)(2,1)} %param.16) | copy-start | bytes 49156
  10.5 4.7 %copy-start.5 = (bf16[128,64]{0,1:T(8,128)(2,1)S(1)}, bf16[128,64]{0,1:T(8,128)(2,1)}, u32[]{:S(2)}) copy-start(bf16[128,64]{0,1:T(8,128)(2,1)} %param.19) | copy-start | bytes 49156
  10.5 4.8 %copy-start.6 = (bf16[64,128]{1,0:T(8,128)(2,1)S(1)}, bf16[64,128]{1,0:T(8,128)(2,1)}, u32[]{:S(2)}) copy-start(bf16[64,128]{1,0:T(8,128)(2,1)} %param.15) | copy-start | bytes 49156
  10.5 4.8 %copy-start.7 = (bf16[64,128]{1,0:T(8,128)(2,1)S(1)}, bf16[64,128]{1,0:T(8,128)(2,1)}, u32[]{:S(2)}) copy-start(bf16[64,128]{1,0:T(8,128)(2,1)} %param.17) | copy-start | bytes 49156
  10.5 117.5 %all-to-all-start = ((bf16[8,384,256]{2,1,0:T(8,128)(2,1)}), bf16[8,384,256]{2,1,0:T(8,128)(2,1)}, u32[]{:S(2)}, u32[]{:S(2)}) async-start(bf16[8,384,256]{2,1,0:T(8,128)(2,1)} %broadcast_in_dim.2), calls=%async_computation | async-start | bytes 3145728 | tf_op jit(solution)/shard_map/all_to_all | solution.py:24
  15.3 112.6 %copy-start.3 = (f32[2048]{0:T(1024)S(1)}, f32[2048]{0:T(1024)}, u32[]{:S(2)}) copy-start(f32[2048]{0:T(1024)} %param.14) | copy-start | bytes 24580
  109.0 30.2 %collective-permute-start = (bf16[2048,128]{1,0:T(8,128)(2,1)S(1)}, bf16[2048,128]{1,0:T(8,128)(2,1)}, u32[]{:S(2)}, u32[]{:S(2)}) collective-permute-start(bf16[2048,128]{1,0:T(8,128)(2,1)S(1)} %bitcast.96), channel_id=1, source_target_pairs={{0,256},{256,0},{1,257},{257,1},{2,258},{258,2},{3,259},{259,3},{4... | collective-permute-start | bytes 1572872 | tf_op jit(solution)/shard_map/ppermute | solution.py:30
  123.5 17.4 %collective-permute-start.1 = (bf16[2048,128]{1,0:T(8,128)(2,1)S(1)}, bf16[2048,128]{1,0:T(8,128)(2,1)S(1)}, u32[]{:S(2)}, u32[]{:S(2)}) collective-permute-start(bf16[2048,128]{1,0:T(8,128)(2,1)S(1)} %bitcast.90), channel_id=1, source_target_pairs={{0,256},{256,0},{1,257},{257,1},{2,258},{258,2},{3,259},{259,3},{4... | collective-permute-start | bytes 1572872 | tf_op jit(solution)/shard_map/ppermute | solution.py:30
  139.2 1.7 copy-start.1
  143.2 4.2 %collective-permute-start.2 = (bf16[4,384,256]{2,1,0:T(8,128)(2,1)S(1)}, bf16[4,384,256]{2,1,0:T(8,128)(2,1)S(1)}, u32[]{:S(2)}, u32[]{:S(2)}) collective-permute-start(bf16[4,384,256]{2,1,0:T(8,128)(2,1)S(1)} %get-tuple-element.8), channel_id=1, source_target_pairs={{0,1},{1,0},{2,3},{3,2},{4,5},{5,4},{6,7},{7,6},{8,9},{9,8},{10,11... | collective-permute-start | bytes 2359304 | tf_op jit(solution)/shard_map/ppermute | solution.py:30
  147.7 18.0 %copy-start.2 = (bf16[384,256]{1,0:T(8,128)(2,1)S(1)}, bf16[384,256]{1,0:T(8,128)(2,1)}, u32[]{:S(2)}) copy-start(bf16[384,256]{1,0:T(8,128)(2,1)} %param.13) | copy-start | bytes 589828
  165.5 16.5 %copy-start.10 = (f32[2,640]{1,0:T(2,128)S(1)}, f32[2,640]{1,0:T(2,128)}, u32[]{:S(2)}) copy-start(f32[2,640]{1,0:T(2,128)} %param.24) | copy-start | bytes 15364
  165.5 16.6 %copy-start.8 = (f32[2,3,640]{2,0,1:T(2,128)S(1)}, f32[2,3,640]{2,0,1:T(2,128)}, u32[]{:S(2)}) copy-start(f32[2,3,640]{2,0,1:T(2,128)} %param.23) | copy-start | bytes 46084
  179.9 4.2 %collective-permute-start.3 = (bf16[4,384,256]{2,1,0:T(8,128)(2,1)S(1)}, bf16[4,384,256]{2,1,0:T(8,128)(2,1)S(1)}, u32[]{:S(2)}, u32[]{:S(2)}) collective-permute-start(bf16[4,384,256]{2,1,0:T(8,128)(2,1)S(1)} %bitcast.94), channel_id=1, source_target_pairs={{0,1},{1,0},{2,3},{3,2},{4,5},{5,4},{6,7},{7,6},{8,9},{9,8},{10,11... | collective-permute-start | bytes 2359304 | tf_op jit(solution)/shard_map/ppermute | solution.py:30
  184.4 0.7 copy-start.9
  190.7 4.0 %copy-start = (bf16[3,2048,640]{2,1,0:T(8,128)(2,1)S(1)}, bf16[3,2048,640]{2,1,0:T(8,128)(2,1)}, u32[]{:S(2)}) copy-start(bf16[3,2048,640]{2,1,0:T(8,128)(2,1)} %all-gather.4.cloned.1.call-done.weights) | copy-start | bytes 23592964
  197.9 4.2 %collective-permute-start.4 = (bf16[4,384,256]{2,1,0:T(8,128)(2,1)S(1)}, bf16[4,384,256]{2,1,0:T(8,128)(2,1)S(1)}, u32[]{:S(2)}, u32[]{:S(2)}) collective-permute-start(bf16[4,384,256]{2,1,0:T(8,128)(2,1)S(1)} %down_terms.3), channel_id=1, source_target_pairs={{0,1},{1,0},{2,3},{3,2},{4,5},{5,4},{6,7},{7,6},{8,9},{9,8},{10,11... | collective-permute-start | bytes 2359304 | tf_op jit(solution)/shard_map/ppermute | solution.py:30
Sparse Core Ops, SparseCore 0:
  9.4 181.2 all-gather.3
